TPU v7x, 32 devices: a whole 2x2x4 slice. The times are simulated.
32 devices in a mesh: fs: 4 (over z), tp: 8 (over y, x, core).
Axes of the slice: x: 2, y: 2, z: 4, core: 2. Of those that a mesh axis runs over, the one named last changes fastest.
Arguments:
- tokens: bfloat16 [1024, 2048], P('fs', 'tp'), may hold values from -6 to 6
- norm_gain: float32 [2048], P('tp'), may hold values from 0.1 to 1.9
- gate_master: float32 [8, 3584, 2048], P(None, 'fs', 'tp'), may hold values from -0.125 to 0.125
- up_master: float32 [8, 3584, 2048], P(None, 'fs', 'tp'), may hold values from -0.125 to 0.125
- down_master: float32 [8, 3584, 2048], P(None, 'fs', 'tp'), may hold values from -0.0625 to 0.0625
- routes: int32 [1024, 2], P('fs'), may hold values from 0 to 3, all different within a row; in each aligned block of 256 rows (0 to 255, 256 to 511, ...) at most 128 rows name the same one
- route_logits: float32 [1024, 2], P('fs'), may hold values from -8 to 8
Outputs:
- gate_serve: bfloat16 [8, 3584, 2048], P('tp', 'fs')
- up_serve: bfloat16 [8, 3584, 2048], P('tp', 'fs')
- down_serve: bfloat16 [8, 3584, 2048], P('tp', 'fs')
- mixed_tokens: bfloat16 [1024, 2048], P('fs', 'tp')
Inputs may be any that keep to these rules, and one draw needn't show every extreme that they name: `routes`: each row names 2 different experts; in every aligned block of 256 rows each expert is named by exactly 128 rows.
All inputs are finite; a program needn't handle non-finite values.
Results may differ from a plain program's by a relative error of at most 0.024.
Values may be sent and summed in bfloat16 or wider, within the bound.
No kernel may reach another device: no remote copies, remote signals or barrier semaphores. Data moves between devices by JAX's collectives and lax.ppermute only.
A program may use at most 128 MiB of HBM per device.

v0:
```python
import functools

import jax
import jax.numpy as jnp
from jax import lax
from jax.experimental import pallas as pl
from jax.experimental.pallas import tpu as pltpu
from jax.sharding import PartitionSpec as P


epsilon = 1e-05


def swap(value, axis, mask):
    if mask == 0:
        return value
    pairs = [(source, source ^ mask) for source in range(lax.axis_size(axis))]
    return lax.ppermute(value, axis, pairs)


def row_tile(rows):
    return rows // 2 if rows > 256 and rows % 32 == 0 else rows


def norm_kernel(me_ref, *refs):
    chunks, out_ref = refs[:-1], refs[-1]
    width = chunks[0].shape[1]
    total = jnp.zeros((chunks[0].shape[0], 1), jnp.float32)
    for ref in chunks:
        wide = ref[...].astype(jnp.float32)
        total = total + jnp.sum(wide * wide, axis=1, keepdims=True)
    scale = lax.rsqrt(total / (width * len(chunks)) + epsilon)
    for mask, ref in enumerate(chunks):
        start = pl.multiple_of((me_ref[0] ^ mask) * width, width)
        out_ref[:, pl.ds(start, width)] = (ref[...].astype(jnp.float32) * scale).astype(
            jnp.bfloat16
        )


def norm_rows(me, chunks):
    rows, width = chunks[0].shape
    return pl.pallas_call(
        norm_kernel,
        out_shape=jax.ShapeDtypeStruct((rows, width * len(chunks)), jnp.bfloat16),
        in_specs=[pl.BlockSpec(memory_space=pltpu.SMEM)]
        + [pl.BlockSpec(memory_space=pltpu.VMEM)] * len(chunks),
        out_specs=pl.BlockSpec(memory_space=pltpu.VMEM),
        cost_estimate=pl.CostEstimate(flops=10**8, bytes_accessed=10**6, transcendentals=0),
        name="norm_rows",
    )(me, *chunks)


def ready_kernel(masks, me_ref, master_ref, *refs):
    count = len(masks)
    outs, held, arrived = refs[-count - 2 : -2], refs[-2], refs[-1]
    gain = refs[0][...] if len(refs) > count + 2 else None
    copies = [
        pltpu.make_async_copy(master_ref.at[me_ref[0] ^ mask], held.at[k], arrived.at[k])
        for k, mask in enumerate(masks)
    ]
    for copy in copies:
        copy.start()
    for k, copy in enumerate(copies):
        copy.wait()
        piece = held[k] if gain is None else held[k] * gain
        outs[k][...] = piece.astype(jnp.bfloat16)


def ready(master, gain, me, masks):
    _, rows, width = master.shape
    count = len(masks)
    in_specs = [pl.BlockSpec(memory_space=pltpu.SMEM), pl.BlockSpec(memory_space=pltpu.HBM)]
    inputs = [me, master]
    if gain is not None:
        in_specs.append(pl.BlockSpec(memory_space=pltpu.VMEM))
        inputs.append(gain[None, :])
    return pl.pallas_call(
        functools.partial(ready_kernel, masks),
        in_specs=in_specs,
        out_specs=[pl.BlockSpec(memory_space=pltpu.VMEM)] * count,
        out_shape=[jax.ShapeDtypeStruct((rows, width), jnp.bfloat16)] * count,
        scratch_shapes=[
            pltpu.VMEM((count, rows, width), jnp.float32),
            pltpu.SemaphoreType.DMA((count,)),
        ],
        compiler_params=pltpu.CompilerParams(vmem_limit_bytes=60 * 2**20),
        cost_estimate=pl.CostEstimate(
            flops=10**8, bytes_accessed=6 * count * rows * width, transcendentals=0
        ),
    )(*inputs)


contract = (((1,), (1,)), ((), ()))


def place(me_ref, pieces, slab_ref):
    width = pieces[0].shape[1]
    for mask, ref in enumerate(pieces):
        start = pl.multiple_of((me_ref[0] ^ mask) * width, width)
        slab_ref[0, :, pl.ds(start, width)] = ref[...]


def gate_kernel(count, me_ref, mine_ref, theirs_ref, *refs):
    pieces, (slab_ref, act_ref) = refs[:count], refs[count:]
    place(me_ref, pieces, slab_ref)
    half = mine_ref.shape[0]
    for number, rows in enumerate((mine_ref, theirs_ref)):
        pre = lax.dot_general(rows[...], slab_ref[0], contract, preferred_element_type=jnp.float32)
        act_ref[0, pl.ds(number * half, half), :] = pre * (1.0 / (1.0 + jnp.exp(-pre)))


def up_kernel(count, me_ref, mine_ref, theirs_ref, act_ref, *refs):
    pieces, (slab_ref, hidden_ref) = refs[:count], refs[count:]
    place(me_ref, pieces, slab_ref)
    half = mine_ref.shape[0]
    for number, rows in enumerate((mine_ref, theirs_ref)):
        part = pl.ds(number * half, half)
        pre = lax.dot_general(rows[...], slab_ref[0], contract, preferred_element_type=jnp.float32)
        hidden_ref[0, part, :] = (act_ref[0, part, :] * pre).astype(jnp.bfloat16)


def fill_kernel(masks, me_ref, *refs):
    count = len(masks)
    pieces, slab_ref, left = refs[:count], refs[-2], refs[-1]
    width = pieces[0].shape[1]
    copies = []
    for k, mask in enumerate(masks):
        start = pl.multiple_of((me_ref[0] ^ mask) * width, width)
        copies.append(
            pltpu.make_async_copy(pieces[k], slab_ref.at[0, :, pl.ds(start, width)], left.at[k])
        )
    for copy in copies:
        copy.start()
    for copy in copies:
        copy.wait()


def fill_call(me, pieces, masks, model, slab):
    rows, width = pieces[0].shape
    count = len(masks)
    in_specs = [pl.BlockSpec(memory_space=pltpu.SMEM)]
    in_specs += [pl.BlockSpec(memory_space=pltpu.VMEM)] * count
    inputs = [me, *pieces]
    if slab is not None:
        in_specs.append(pl.BlockSpec(memory_space=pl.ANY))
        inputs.append(slab)
    return pl.pallas_call(
        functools.partial(fill_kernel, masks),
        in_specs=in_specs,
        out_specs=pl.BlockSpec(memory_space=pl.ANY),
        out_shape=jax.ShapeDtypeStruct((1, rows, model), jnp.bfloat16),
        input_output_aliases={} if slab is None else {1 + count: 0},
        scratch_shapes=[pltpu.SemaphoreType.DMA((count,))],
        compiler_params=pltpu.CompilerParams(vmem_limit_bytes=52 * 2**20),
        cost_estimate=pl.CostEstimate(
            flops=10**8, bytes_accessed=4 * count * rows * width, transcendentals=0
        ),
    )(*inputs)


def slab_call(kernel, me, wide, act, pieces, out_type):
    block_rows, width = pieces[0].shape
    model = width * len(pieces)
    tile = row_tile(block_rows)
    rows = sum(value.shape[0] for value in wide)
    in_specs = [pl.BlockSpec(value.shape, lambda t, me: (0, 0)) for value in wide]
    if act is not None:
        in_specs.append(pl.BlockSpec((1, rows, tile), lambda t, me: (t, 0, 0)))
    in_specs += [pl.BlockSpec((tile, width), lambda t, me: (t, 0))] * len(pieces)
    out_specs = [pl.BlockSpec((1, tile, model), lambda t, me: (0, t, 0))]
    out_shape = [jax.ShapeDtypeStruct((1, block_rows, model), jnp.bfloat16)]
    if out_type is not None:
        out_specs.append(pl.BlockSpec((1, rows, tile), lambda t, me: (t, 0, 0)))
        out_shape.append(jax.ShapeDtypeStruct((block_rows // tile, rows, tile), out_type))
    return pl.pallas_call(
        functools.partial(kernel, len(pieces)),
        grid_spec=pltpu.PrefetchScalarGridSpec(
            num_scalar_prefetch=1,
            grid=(block_rows // tile,),
            in_specs=in_specs,
            out_specs=out_specs,
        ),
        out_shape=out_shape,
        compiler_params=pltpu.CompilerParams(vmem_limit_bytes=52 * 2**20),
        cost_estimate=pl.CostEstimate(
            flops=2 * rows * block_rows * model + 10**8,
            bytes_accessed=4 * block_rows * model,
            transcendentals=0,
        ),
    )(me, *wide, *(() if act is None else (act,)), *pieces)


def dots_kernel(count, hidden_ref, *refs):
    pieces, (sent_ref, own_ref) = refs[:count], refs[count:]
    blocks, _, rows, width = own_ref.shape
    half = blocks * rows
    tiles, _, tile = hidden_ref.shape
    for number, ref in enumerate(pieces):
        for target, slot, start in ((sent_ref, number ^ 1, half), (own_ref, number, 0)):
            out = sum(
                jnp.dot(
                    hidden_ref[t, start : start + half],
                    ref[t * tile : (t + 1) * tile],
                    preferred_element_type=jnp.float32,
                )
                for t in range(tiles)
            )
            target[:, slot] = out.reshape(blocks, rows, width)


def dots_call(hidden, pieces, blocks):
    rows = hidden.shape[1]
    inner, width = pieces[0].shape
    out = jax.ShapeDtypeStruct((blocks, len(pieces), rows // 2 // blocks, width), jnp.float32)
    return pl.pallas_call(
        functools.partial(dots_kernel, len(pieces)),
        in_specs=[pl.BlockSpec(memory_space=pltpu.VMEM)] * (1 + len(pieces)),
        out_specs=[pl.BlockSpec(memory_space=pltpu.VMEM)] * 2,
        out_shape=[out, out],
        compiler_params=pltpu.CompilerParams(vmem_limit_bytes=52 * 2**20),
        cost_estimate=pl.CostEstimate(
            flops=2 * rows * inner * width * len(pieces) + 10**8,
            bytes_accessed=2 * inner * width * len(pieces),
            transcendentals=0,
        ),
    )(hidden, *pieces)


def local(tokens, norm_gain, gate_master, up_master, down_master, routes, route_logits):
    tok_rows = tokens.shape[0]
    slabs = lax.axis_size("tp")
    blocks = lax.axis_size("fs")
    experts = slabs // 2
    capacity = tok_rows * routes.shape[1] // experts
    half_cap = capacity // 2
    me = lax.axis_index("tp")
    me_ref = me.astype(jnp.int32)[None]

    def deliver(master, gain, groups):
        got = {}
        for masks in groups:
            pieces = ready(master, gain, me_ref, masks)
            for mask, piece in zip(masks, pieces):
                got[mask] = swap(piece, "tp", mask)
        return [got[mask] for mask in range(slabs)]

    first_groups, groups = piece_groups(slabs)
    gate_pieces = deliver(gate_master, norm_gain, first_groups)

    first_prob = jax.nn.sigmoid(route_logits[:, 0] - route_logits[:, 1])
    choice_prob = jnp.stack([first_prob, 1.0 - first_prob], axis=1)
    expert_ids = jnp.arange(experts, dtype=jnp.int32)
    matches = (routes[:, :, None] == expert_ids[None, None, :]).astype(jnp.float32)
    chosen = jnp.sum(matches, axis=1)
    weight = jnp.sum(matches * choice_prob[:, :, None], axis=1)
    position = jnp.cumsum(chosen, axis=0) - 1.0
    slot_ids = jnp.arange(capacity, dtype=jnp.float32)
    placed = chosen.T[:, None, :] * (position.T[:, None, :] == slot_ids[None, :, None]).astype(
        jnp.float32
    )
    placed = placed.astype(jnp.bfloat16)
    by_slab = placed.reshape(slabs, half_cap, tok_rows)
    spread = [
        jnp.concatenate([lax.dynamic_index_in_dim(by_slab, me ^ m, 0, False) for m in (2 * p, 2 * p + 1)])
        for p in range(experts)
    ]
    share = [lax.dynamic_index_in_dim(weight, (me // 2) ^ p, 1) for p in range(experts)]
    picked = jnp.dot(
        placed.reshape(experts * capacity, tok_rows), tokens, preferred_element_type=jnp.float32
    )
    picked = picked.astype(jnp.bfloat16).reshape(slabs, half_cap, tokens.shape[1])
    chunks = [
        swap(lax.dynamic_index_in_dim(picked, me ^ m, 0, keepdims=False), "tp", m)
        for m in range(slabs)
    ]
    normed = norm_rows(me_ref, chunks)
    direct = blocks <= 8
    if direct:
        gathered = [swap(normed, "fs", z) for z in range(blocks)]
        mine = jnp.concatenate(gathered, axis=0)
    else:
        mine = lax.all_gather(normed, "fs", axis=0, tiled=True)
    theirs = swap(mine, "tp", 1)

    up_pieces = deliver(up_master, norm_gain, groups)
    down_pieces = deliver(down_master, None, groups)

    gate_serve, act = slab_call(gate_kernel, me_ref, (mine, theirs), None, gate_pieces, jnp.float32)
    up_serve, hidden = slab_call(up_kernel, me_ref, (mine, theirs), act, up_pieces, jnp.bfloat16)
    backs = {}
    down_serve = None
    pairs = pair_groups(experts)
    for number, group in enumerate(pairs):
        masks = [mask for pair in group for mask in (2 * pair, 2 * pair + 1)]
        sent, own = dots_call(hidden, [down_pieces[m] for m in masks], blocks)
        got = swap(sent, "tp", 1)
        parts = [(own[z] + got[z]).astype(jnp.bfloat16) for z in range(blocks)]
        if direct:
            parts = [swap(part, "fs", z) for z, part in enumerate(parts)]
        else:
            parts = lax.all_to_all(jnp.stack(parts), "fs", split_axis=0, concat_axis=0, tiled=True)
        for k, mask in enumerate(masks):
            total = sum(parts[z][k].astype(jnp.float32) for z in range(blocks))
            total = total.astype(jnp.bfloat16)
            backs[mask] = swap(total, "tp", mask)
        if number > 0:
            filled = masks if number > 1 else [0, 1] + masks
            pieces = [down_pieces[m] for m in filled]
            model = down_pieces[0].shape[1] * slabs
            down_serve = fill_call(me_ref, pieces, filled, model, down_serve)

    mixed = jnp.zeros((tok_rows, tokens.shape[1]), jnp.float32)
    for pair in range(experts):
        rows = jnp.concatenate([backs[2 * pair], backs[2 * pair + 1]])
        term = lax.dot_general(
            spread[pair], rows, (((0,), (0,)), ((), ())), preferred_element_type=jnp.float32
        )
        mixed = mixed + share[pair] * term

    return (gate_serve, up_serve, down_serve, mixed.astype(jnp.bfloat16))


def piece_groups(slabs):
    order = [mask for mask in (4, 2, 5, 3, 6, 7, *range(8, slabs)) if mask < slabs] + [1, 0]
    return [order[:2], order[2:]], [order]


def pair_groups(experts):
    return [[0], [*range(1, experts - 1)], [experts - 1]]


def solution(mesh):
    placed = (
        P("fs", "tp"),
        P("tp"),
        P(None, "fs", "tp"),
        P(None, "fs", "tp"),
        P(None, "fs", "tp"),
        P("fs", None),
        P("fs", None),
    )
    return jax.shard_map(
        local,
        mesh=mesh,
        in_specs=placed,
        out_specs=(P("tp", "fs", None), P("tp", "fs", None), P("tp", "fs", None), P("fs", "tp")),
        check_vma=False,
    )
```

profile of v0, /device:TPU:1, one launch (start us, length us, event | category | flops | bytes accessed | tf_op | source)
XLA Modules:
  0.0 216.7 jit_solution(3242253924811511940)
XLA Ops:
  4.9 2.7 %collective-permute-start.1 = (bf16[64,256]{1,0:T(8,128)(2,1)S(1)}, bf16[64,256]{1,0:T(8,128)(2,1)S(1)}, u32[]{:S(2)}, u32[]{:S(2)}) collective-permute-start(bf16[64,256]{1,0:T(8,128)(2,1)S(1)} %get-tuple-element.109), channel_id=1, source_target_pairs={{0,2},{1,3},{2,0},{3,1},{4,6},{5,7},{6,4},{7,5},{8,10},{9,11},{10,... | collective-permute-start | bytes 98312 | tf_op jit(solution)/shard_map/ppermute | solution.py:18
  9.6 2.4 %collective-permute-start.5 = (bf16[64,256]{1,0:T(8,128)(2,1)S(1)}, bf16[64,256]{1,0:T(8,128)(2,1)S(1)}, u32[]{:S(2)}, u32[]{:S(2)}) collective-permute-start(bf16[64,256]{1,0:T(8,128)(2,1)S(1)} %get-tuple-element.105), channel_id=1, source_target_pairs={{0,6},{1,7},{2,4},{3,5},{4,2},{5,3},{6,0},{7,1},{8,14},{9,15},{10,... | collective-permute-start | bytes 98312 | tf_op jit(solution)/shard_map/ppermute | solution.py:18
  13.3 2.9 %collective-permute-done.6.refs_7_ = bf16[64,256]{1,0:T(8,128)(2,1)S(1)} collective-permute-done((bf16[64,256]{1,0:T(8,128)(2,1)S(1)}, bf16[64,256]{1,0:T(8,128)(2,1)S(1)}, u32[]{:S(2)}, u32[]{:S(2)}) %collective-permute-start.6) | collective-permute-done | bytes 32800 | tf_op jit(solution)/shard_map/ppermute | solution.py:18
  19.9 4.9 %shard_map.102 = (bf16[896,256]{1,0:T(8,128)(2,1)}, bf16[896,256]{1,0:T(8,128)(2,1)}, bf16[896,256]{1,0:T(8,128)(2,1)}, bf16[896,256]{1,0:T(8,128)(2,1)}, bf16[8...) custom-call(s32[1]{0:T(128)} %bitcast.me_ref, f32[8,896,256]{2,1,0:T(8,128)} %master_ref.5, f32[1,256]{1,0:T(1,128)} %bitcast.140), custom_call_target="tpu_custom_call" | custom-call | flops 100000000 | bytes 8257536 | tf_op jit(solution)/shard_map/pallas_call | solution.py:77
  26.8 2.3 %collective-permute-start.8 = (bf16[64,2048]{1,0:T(8,128)(2,1)S(1)}, bf16[64,2048]{1,0:T(8,128)(2,1)S(1)}, u32[]{:S(2)}, u32[]{:S(2)}) collective-permute-start(bf16[64,2048]{1,0:T(8,128)(2,1)S(1)} %copy-done.22), channel_id=1, source_target_pairs={{0,16},{8,24},{16,0},{24,8},{1,17},{9,25},{17,1},{25,9},{2,18},{10... | collective-permute-start | bytes 786440 | tf_op jit(solution)/shard_map/ppermute | solution.py:18
  29.8 17.4 %collective-permute-done.8 = bf16[64,2048]{1,0:T(8,128)(2,1)S(1)} collective-permute-done((bf16[64,2048]{1,0:T(8,128)(2,1)S(1)}, bf16[64,2048]{1,0:T(8,128)(2,1)S(1)}, u32[]{:S(2)}, u32[]{:S(2)}) %collective-permute-start.8) | collective-permute-done | bytes 262176 | tf_op jit(solution)/shard_map/ppermute | solution.py:18
  48.7 3.1 %shard_map.103 = (bf16[896,256]{1,0:T(8,128)(2,1)}, bf16[896,256]{1,0:T(8,128)(2,1)}) custom-call(s32[1]{0:T(128)} %bitcast.me_ref, f32[8,896,256]{2,1,0:T(8,128)} %master_ref.5, f32[1,256]{1,0:T(1,128)} %bitcast.141), custom_call_target="tpu_custom_call" | custom-call | flops 100000000 | bytes 2752512 | tf_op jit(solution)/shard_map/pallas_call | solution.py:77
  55.2 5.7 %shard_map.105 = (bf16[896,256]{1,0:T(8,128)(2,1)}, bf16[896,256]{1,0:T(8,128)(2,1)}, bf16[896,256]{1,0:T(8,128)(2,1)}, bf16[896,256]{1,0:T(8,128)(2,1)}, bf16[8...) custom-call(s32[1]{0:T(128)} %bitcast.me_ref, ...), custom_call_target="tpu_custom_call" | custom-call | flops 100000000 | bytes 11010048 | tf_op jit(solution)/shard_map/pallas_call | solution.py:77
  62.6 8.8 %collective-permute-done.17.refs_7_ = bf16[896,256]{1,0:T(8,128)(2,1)} collective-permute-done((bf16[896,256]{1,0:T(8,128)(2,1)S(1)}, bf16[896,256]{1,0:T(8,128)(2,1)}, u32[]{:S(2)}, u32[]{:S(2)}) %collective-permute-start.17) | collective-permute-done | bytes 458784 | tf_op jit(solution)/shard_map/ppermute | solution.py:18
  72.0 7.1 %collective-permute-done.12.refs_2_ = bf16[896,256]{1,0:T(8,128)(2,1)S(1)} collective-permute-done((bf16[896,256]{1,0:T(8,128)(2,1)}, bf16[896,256]{1,0:T(8,128)(2,1)S(1)}, u32[]{:S(2)}, u32[]{:S(2)}) %collective-permute-start.12) | collective-permute-done | bytes 458784 | tf_op jit(solution)/shard_map/ppermute | solution.py:18
  79.9 3.3 %collective-permute-start.20 = (bf16[896,256]{1,0:T(8,128)(2,1)}, bf16[896,256]{1,0:T(8,128)(2,1)S(1)}, u32[]{:S(2)}, u32[]{:S(2)}) collective-permute-start(bf16[896,256]{1,0:T(8,128)(2,1)} %get-tuple-element.51), channel_id=1, source_target_pairs={{0,3},{1,2},{2,1},{3,0},{4,7},{5,6},{6,5},{7,4},{8,11},{9,10},{10,... | collective-permute-start | bytes 1376264 | tf_op jit(solution)/shard_map/ppermute | solution.py:18
  83.7 5.0 %shard_map.107 = (bf16[896,256]{1,0:T(8,128)(2,1)}, bf16[896,256]{1,0:T(8,128)(2,1)}, bf16[896,256]{1,0:T(8,128)(2,1)}, bf16[896,256]{1,0:T(8,128)(2,1)}, bf16[8...) custom-call(s32[1]{0:T(128)} %bitcast.me_ref, ...), custom_call_target="tpu_custom_call" | custom-call | flops 100000000 | bytes 11010048 | tf_op jit(solution)/shard_map/pallas_call | solution.py:77
  90.7 9.8 %collective-permute-done.20.refs_3_ = bf16[896,256]{1,0:T(8,128)(2,1)S(1)} collective-permute-done((bf16[896,256]{1,0:T(8,128)(2,1)}, bf16[896,256]{1,0:T(8,128)(2,1)S(1)}, u32[]{:S(2)}, u32[]{:S(2)}) %collective-permute-start.20) | collective-permute-done | bytes 458784 | tf_op jit(solution)/shard_map/ppermute | solution.py:18
  103.7 20.5 %collective-permute-done.22.refs_5_ = bf16[896,256]{1,0:T(8,128)(2,1)S(1)} collective-permute-done((bf16[896,256]{1,0:T(8,128)(2,1)}, bf16[896,256]{1,0:T(8,128)(2,1)S(1)}, u32[]{:S(2)}, u32[]{:S(2)}) %collective-permute-start.22) | collective-permute-done | bytes 458784 | tf_op jit(solution)/shard_map/ppermute | solution.py:18
  128.9 6.5 %collective-permute-done.28.refs_2_.refs_0_ = bf16[896,256]{1,0:T(8,128)(2,1)S(1)} collective-permute-done((bf16[896,256]{1,0:T(8,128)(2,1)}, bf16[896,256]{1,0:T(8,128)(2,1)S(1)}, u32[]{:S(2)}, u32[]{:S(2)}) %collective-permute-start.28) | collective-permute-done | bytes 458784 | tf_op jit(solution)/shard_map/ppermute | solution.py:18
  135.4 1.9 collective-permute-start.25
  137.3 4.0 %collective-permute-start.26 = (bf16[896,256]{1,0:T(8,128)(2,1)}, bf16[896,256]{1,0:T(8,128)(2,1)S(1)}, u32[]{:S(2)}, u32[]{:S(2)}) collective-permute-start(bf16[896,256]{1,0:T(8,128)(2,1)} %get-tuple-element.58), channel_id=1, source_target_pairs={{0,7},{1,6},{2,5},{3,4},{4,3},{5,2},{6,1},{7,0},{8,15},{9,14},{10,... | collective-permute-start | bytes 1376264 | tf_op jit(solution)/shard_map/ppermute | solution.py:18
  144.3 6.6 %shard_map.104 = (bf16[1,896,2048]{2,1,0:T(8,128)(2,1)}, f32[2,512,448]{2,1,0:T(8,128)}) custom-call(s32[1]{0:T(128)} %bitcast.me_ref, bf16[256,2048]{1,0:T(8,128)(2,1)} %pad_maximum_fusion.mine_ref, bf16[256,2048]{1,0:T(8,128)(2,1)} %collective-permute-done.10.theirs_ref, bf16[896,256]{1,0:T(8,128)(2,1)S(1)} %copy-done.14, bf16[896,256]{1,0:T(8,128)(2,1)S(1)} %copy-done.16, ...), custom_call_target="tpu_custom_call" | custom-call | flops 1979048192 | bytes 7340032 | tf_op jit(solution)/shard_map/pallas_call | solution.py:175
  151.0 6.7 %shard_map.106 = (bf16[1,896,2048]{2,1,0:T(8,128)(2,1)}, bf16[2,512,448]{2,1,0:T(8,128)(2,1)}) custom-call(s32[1]{0:T(128)} %bitcast.me_ref, bf16[256,2048]{1,0:T(8,128)(2,1)} %pad_maximum_fusion.mine_ref, bf16[256,2048]{1,0:T(8,128)(2,1)} %collective-permute-done.10.theirs_ref, f32[2,512,448]{2,1,0:T(8,128)} %get-tuple-element.47.act_ref, ...), custom_call_target="tpu_custom_call" | custom-call | flops 1979048192 | bytes 7340032 | tf_op jit(solution)/shard_map/pallas_call | solution.py:175
  157.7 2.7 %shard_map.110 = (f32[4,2,64,256]{3,2,1,0:T(8,128)}, f32[4,2,64,256]{3,2,1,0:T(8,128)S(1)}) custom-call(bf16[2,512,448]{2,1,0:T(8,128)(2,1)} %get-tuple-element.65.hidden_ref, bf16[896,256]{1,0:T(8,128)(2,1)S(1)} %copy-done.2, bf16[896,256]{1,0:T(8,128)(2,1)S(1)} %collective-permute-done.27.refs_1_), custom_call_target="tpu_custom_call" | custom-call | flops 569762048 | bytes 917504 | tf_op jit(solution)/shard_map/pallas_call | solution.py:215
  160.5 8.7 %collective-permute-done.31.refs_5_.refs_3_ = bf16[896,256]{1,0:T(8,128)(2,1)S(1)} collective-permute-done((bf16[896,256]{1,0:T(8,128)(2,1)}, bf16[896,256]{1,0:T(8,128)(2,1)S(1)}, u32[]{:S(2)}, u32[]{:S(2)}) %collective-permute-start.31) | collective-permute-done | bytes 458784 | tf_op jit(solution)/shard_map/ppermute | solution.py:18
  169.2 4.0 %shard_map.111 = (f32[4,4,64,256]{3,2,1,0:T(8,128)}, f32[4,4,64,256]{3,2,1,0:T(8,128)}) custom-call(bf16[2,512,448]{2,1,0:T(8,128)(2,1)} %get-tuple-element.65.hidden_ref, bf16[896,256]{1,0:T(8,128)(2,1)S(1)} %collective-permute-done.28.refs_2_.refs_0_, bf16[896,256]{1,0:T(8,128)(2,1)S(1)} %collective-permute-done.29.refs_3_.refs_1_, ...), custom_call_target="tpu_custom_call" | custom-call | flops 1039524096 | bytes 1835008 | tf_op jit(solution)/shard_map/pallas_call | solution.py:215
  173.9 3.1 %shard_map.112 = (f32[4,2,64,256]{3,2,1,0:T(8,128)}, f32[4,2,64,256]{3,2,1,0:T(8,128)S(1)}) custom-call(bf16[2,512,448]{2,1,0:T(8,128)(2,1)} %get-tuple-element.65.hidden_ref, bf16[896,256]{1,0:T(8,128)(2,1)S(1)} %collective-permute-done.25.refs_0_, bf16[896,256]{1,0:T(8,128)(2,1)S(1)} %collective-permute-done.26.refs_1_), custom_call_target="tpu_custom_call" | custom-call | flops 569762048 | bytes 917504 | tf_op jit(solution)/shard_map/pallas_call | solution.py:215
  177.3 2.8 %shard_map.108.refs_2_ = bf16[1,896,2048]{2,1,0:T(8,128)(2,1)} custom-call(s32[1]{0:T(128)} %bitcast.me_ref, bf16[896,256]{1,0:T(8,128)(2,1)S(1)} %copy-done.2, bf16[896,256]{1,0:T(8,128)(2,1)S(1)} %collective-permute-done.27.refs_1_, bf16[896,256]{1,0:T(8,128)(2,1)S(1)} %collective-permute-done.28.refs_2_.refs_0_, ...), custom_call_target="tpu_custom_call" | custom-call | flops 100000000 | bytes 5505024 | tf_op jit(solution)/shard_map/pallas_call | solution.py:147
  182.4 3.1 %collective-permute-start.34 = (bf16[2,64,256]{2,1,0:T(8,128)(2,1)S(1)}, bf16[2,64,256]{2,1,0:T(8,128)(2,1)S(1)}, u32[]{:S(2)}, u32[]{:S(2)}) collective-permute-start(bf16[2,64,256]{2,1,0:T(8,128)(2,1)S(1)} %get-tuple-element.82), channel_id=1, source_target_pairs={{0,16},{8,24},{16,0},{24,8},{1,17},{9,25},{17,1},{25,9},{2,18},{10... | collective-permute-start | bytes 196616 | tf_op jit(solution)/shard_map/ppermute | solution.py:18
  187.2 3.1 %collective-permute-start.47 = (bf16[2,64,256]{2,1,0:T(8,128)(2,1)S(1)}, bf16[2,64,256]{2,1,0:T(8,128)(2,1)S(1)}, u32[]{:S(2)}, u32[]{:S(2)}) collective-permute-start(bf16[2,64,256]{2,1,0:T(8,128)(2,1)S(1)} %get-tuple-element.86), channel_id=1, source_target_pairs={{0,16},{8,24},{16,0},{24,8},{1,17},{9,25},{17,1},{25,9},{2,18},{10... | collective-permute-start | bytes 196616 | tf_op jit(solution)/shard_map/ppermute | solution.py:18
  190.8 3.9 %collective-permute-start.36 = (bf16[64,256]{1,0:T(8,128)(2,1)S(1)}, bf16[64,256]{1,0:T(8,128)(2,1)S(1)}, u32[]{:S(2)}, u32[]{:S(2)}) collective-permute-start(bf16[64,256]{1,0:T(8,128)(2,1)S(1)} %get-tuple-element.93), channel_id=1, source_target_pairs={{0,1},{1,0},{2,3},{3,2},{4,5},{5,4},{6,7},{7,6},{8,9},{9,8},{10,11... | collective-permute-start | bytes 98312 | tf_op jit(solution)/shard_map/ppermute | solution.py:18
  197.9 1.8 collective-permute-start.40
  201.4 2.6 %collective-permute-done.38 = bf16[4,64,256]{2,1,0:T(8,128)(2,1)S(1)} collective-permute-done((bf16[4,64,256]{2,1,0:T(8,128)(2,1)S(1)}, bf16[4,64,256]{2,1,0:T(8,128)(2,1)S(1)}, u32[]{:S(2)}, u32[]{:S(2)}) %collective-permute-start.38) | collective-permute-done | bytes 131104 | tf_op jit(solution)/shard_map/ppermute | solution.py:18
  203.9 2.3 %collective-permute-start.50 = (bf16[64,256]{1,0:T(8,128)(2,1)S(1)}, bf16[64,256]{1,0:T(8,128)(2,1)S(1)}, u32[]{:S(2)}, u32[]{:S(2)}) collective-permute-start(bf16[64,256]{1,0:T(8,128)(2,1)S(1)} %get-tuple-element.103), channel_id=1, source_target_pairs={{0,7},{1,6},{2,5},{3,4},{4,3},{5,2},{6,1},{7,0},{8,15},{9,14},{10,... | collective-permute-start | bytes 98312 | tf_op jit(solution)/shard_map/ppermute | solution.py:18
  206.3 1.9 collective-permute-done.40
  209.0 2.0 collective-permute-start.42
  (192 shorter events, 51.9 us)
Async XLA Ops:
  18.6 10.5 %collective-permute-start.7 = (bf16[64,2048]{1,0:T(8,128)(2,1)}, bf16[64,2048]{1,0:T(8,128)(2,1)S(1)}, u32[]{:S(2)}, u32[]{:S(2)}) collective-permute-start(bf16[64,2048]{1,0:T(8,128)(2,1)} %norm_rows.1), channel_id=1, source_target_pairs={{0,8},{8,0},{16,24},{24,16},{1,9},{9,1},{17,25},{25,17},{2,10},{10... | collective-permute-start | bytes 786440 | tf_op jit(solution)/shard_map/ppermute | solution.py:18
  24.8 28.5 %collective-permute-start.11 = (bf16[896,256]{1,0:T(8,128)(2,1)}, bf16[896,256]{1,0:T(8,128)(2,1)S(1)}, u32[]{:S(2)}, u32[]{:S(2)}) collective-permute-start(bf16[896,256]{1,0:T(8,128)(2,1)} %get-tuple-element.39), channel_id=1, source_target_pairs={{0,1},{1,0},{2,3},{3,2},{4,5},{5,4},{6,7},{7,6},{8,9},{9,8},{10,11... | collective-permute-start | bytes 1376264 | tf_op jit(solution)/shard_map/ppermute | solution.py:18
  25.5 28.5 %collective-permute-start.13 = (bf16[896,256]{1,0:T(8,128)(2,1)}, bf16[896,256]{1,0:T(8,128)(2,1)S(1)}, u32[]{:S(2)}, u32[]{:S(2)}) collective-permute-start(bf16[896,256]{1,0:T(8,128)(2,1)} %get-tuple-element.41), channel_id=1, source_target_pairs={{0,3},{1,2},{2,1},{3,0},{4,7},{5,6},{6,5},{7,4},{8,11},{9,10},{10,... | collective-permute-start | bytes 1376264 | tf_op jit(solution)/shard_map/ppermute | solution.py:18
  25.7 35.2 %collective-permute-start.15 = (bf16[896,256]{1,0:T(8,128)(2,1)}, bf16[896,256]{1,0:T(8,128)(2,1)S(1)}, u32[]{:S(2)}, u32[]{:S(2)}) collective-permute-start(bf16[896,256]{1,0:T(8,128)(2,1)} %get-tuple-element.43), channel_id=1, source_target_pairs={{0,5},{1,4},{2,7},{3,6},{4,1},{5,0},{6,3},{7,2},{8,13},{9,12},{10,... | collective-permute-start | bytes 1376264 | tf_op jit(solution)/shard_map/ppermute | solution.py:18
  26.8 20.3 %collective-permute-start.8 = (bf16[64,2048]{1,0:T(8,128)(2,1)S(1)}, bf16[64,2048]{1,0:T(8,128)(2,1)S(1)}, u32[]{:S(2)}, u32[]{:S(2)}) collective-permute-start(bf16[64,2048]{1,0:T(8,128)(2,1)S(1)} %copy-done.22), channel_id=1, source_target_pairs={{0,16},{8,24},{16,0},{24,8},{1,17},{9,25},{17,1},{25,9},{2,18},{10... | collective-permute-start | bytes 786440 | tf_op jit(solution)/shard_map/ppermute | solution.py:18
  29.1 22.7 %collective-permute-start.9 = (bf16[64,2048]{1,0:T(8,128)(2,1)S(1)}, bf16[64,2048]{1,0:T(8,128)(2,1)S(1)}, u32[]{:S(2)}, u32[]{:S(2)}) collective-permute-start(bf16[64,2048]{1,0:T(8,128)(2,1)S(1)} %copy-done.22), channel_id=1, source_target_pairs={{0,24},{8,16},{16,8},{24,0},{1,25},{9,17},{17,9},{25,1},{2,26},{10... | collective-permute-start | bytes 786440 | tf_op jit(solution)/shard_map/ppermute | solution.py:18
  47.1 15.3 %collective-permute-start.16 = (bf16[896,256]{1,0:T(8,128)(2,1)}, bf16[896,256]{1,0:T(8,128)(2,1)S(1)}, u32[]{:S(2)}, u32[]{:S(2)}) collective-permute-start(bf16[896,256]{1,0:T(8,128)(2,1)} %get-tuple-element.44), channel_id=1, source_target_pairs={{0,6},{1,7},{2,4},{3,5},{4,2},{5,3},{6,0},{7,1},{8,14},{9,15},{10,... | collective-permute-start | bytes 1376264 | tf_op jit(solution)/shard_map/ppermute | solution.py:18
  51.8 19.6 %collective-permute-start.17 = (bf16[896,256]{1,0:T(8,128)(2,1)S(1)}, bf16[896,256]{1,0:T(8,128)(2,1)}, u32[]{:S(2)}, u32[]{:S(2)}) collective-permute-start(bf16[896,256]{1,0:T(8,128)(2,1)S(1)} %copy-done.36), channel_id=1, source_target_pairs={{0,7},{1,6},{2,5},{3,4},{4,3},{5,2},{6,1},{7,0},{8,15},{9,14},{10,... | collective-permute-start | bytes 1376264 | tf_op jit(solution)/shard_map/ppermute | solution.py:18
  53.3 25.8 %collective-permute-start.12 = (bf16[896,256]{1,0:T(8,128)(2,1)}, bf16[896,256]{1,0:T(8,128)(2,1)S(1)}, u32[]{:S(2)}, u32[]{:S(2)}) collective-permute-start(bf16[896,256]{1,0:T(8,128)(2,1)} %get-tuple-element.40), channel_id=1, source_target_pairs={{0,2},{1,3},{2,0},{3,1},{4,6},{5,7},{6,4},{7,5},{8,10},{9,11},{10,... | collective-permute-start | bytes 1376264 | tf_op jit(solution)/shard_map/ppermute | solution.py:18
  53.9 29.2 %collective-permute-start.14 = (bf16[896,256]{1,0:T(8,128)(2,1)}, bf16[896,256]{1,0:T(8,128)(2,1)}, u32[]{:S(2)}, u32[]{:S(2)}) collective-permute-start(bf16[896,256]{1,0:T(8,128)(2,1)} %get-tuple-element.42), channel_id=1, source_target_pairs={{0,4},{1,5},{2,6},{3,7},{4,0},{5,1},{6,2},{7,3},{8,12},{9,13},{10,... | collective-permute-start | bytes 1376264 | tf_op jit(solution)/shard_map/ppermute | solution.py:18
  60.9 22.4 %collective-permute-start.18 = (bf16[896,256]{1,0:T(8,128)(2,1)}, bf16[896,256]{1,0:T(8,128)(2,1)S(1)}, u32[]{:S(2)}, u32[]{:S(2)}) collective-permute-start(bf16[896,256]{1,0:T(8,128)(2,1)} %get-tuple-element.49), channel_id=1, source_target_pairs={{0,1},{1,0},{2,3},{3,2},{4,5},{5,4},{6,7},{7,6},{8,9},{9,8},{10,11... | collective-permute-start | bytes 1376264 | tf_op jit(solution)/shard_map/ppermute | solution.py:18
  62.4 74.8 %collective-permute-start.10 = (bf16[256,2048]{1,0:T(8,128)(2,1)}, bf16[256,2048]{1,0:T(8,128)(2,1)}, u32[]{:S(2)}, u32[]{:S(2)}) collective-permute-start(bf16[256,2048]{1,0:T(8,128)(2,1)} %pad_maximum_fusion.mine_ref), channel_id=1, source_target_pairs={{0,1},{1,0},{2,3},{3,2},{4,5},{5,4},{6,7},{7,6},{8,9},{9,8},{10,11... | collective-permute-start | bytes 3145736 | tf_op jit(solution)/shard_map/ppermute | solution.py:18
  71.4 17.4 %collective-permute-start.19 = (bf16[896,256]{1,0:T(8,128)(2,1)}, bf16[896,256]{1,0:T(8,128)(2,1)S(1)}, u32[]{:S(2)}, u32[]{:S(2)}) collective-permute-start(bf16[896,256]{1,0:T(8,128)(2,1)} %get-tuple-element.50), channel_id=1, source_target_pairs={{0,2},{1,3},{2,0},{3,1},{4,6},{5,7},{6,4},{7,5},{8,10},{9,11},{10,... | collective-permute-start | bytes 1376264 | tf_op jit(solution)/shard_map/ppermute | solution.py:18
  79.9 20.7 %collective-permute-start.20 = (bf16[896,256]{1,0:T(8,128)(2,1)}, bf16[896,256]{1,0:T(8,128)(2,1)S(1)}, u32[]{:S(2)}, u32[]{:S(2)}) collective-permute-start(bf16[896,256]{1,0:T(8,128)(2,1)} %get-tuple-element.51), channel_id=1, source_target_pairs={{0,3},{1,2},{2,1},{3,0},{4,7},{5,6},{6,5},{7,4},{8,11},{9,10},{10,... | collective-permute-start | bytes 1376264 | tf_op jit(solution)/shard_map/ppermute | solution.py:18
  83.1 18.4 %collective-permute-start.21 = (bf16[896,256]{1,0:T(8,128)(2,1)}, bf16[896,256]{1,0:T(8,128)(2,1)S(1)}, u32[]{:S(2)}, u32[]{:S(2)}) collective-permute-start(bf16[896,256]{1,0:T(8,128)(2,1)} %get-tuple-element.52), channel_id=1, source_target_pairs={{0,4},{1,5},{2,6},{3,7},{4,0},{5,1},{6,2},{7,3},{8,12},{9,13},{10,... | collective-permute-start | bytes 1376264 | tf_op jit(solution)/shard_map/ppermute | solution.py:18
  83.4 40.7 %collective-permute-start.22 = (bf16[896,256]{1,0:T(8,128)(2,1)}, bf16[896,256]{1,0:T(8,128)(2,1)S(1)}, u32[]{:S(2)}, u32[]{:S(2)}) collective-permute-start(bf16[896,256]{1,0:T(8,128)(2,1)} %get-tuple-element.53), channel_id=1, source_target_pairs={{0,5},{1,4},{2,7},{3,6},{4,1},{5,0},{6,3},{7,2},{8,13},{9,12},{10,... | collective-permute-start | bytes 1376264 | tf_op jit(solution)/shard_map/ppermute | solution.py:18
  89.6 35.8 %collective-permute-start.23 = (bf16[896,256]{1,0:T(8,128)(2,1)}, bf16[896,256]{1,0:T(8,128)(2,1)S(1)}, u32[]{:S(2)}, u32[]{:S(2)}) collective-permute-start(bf16[896,256]{1,0:T(8,128)(2,1)} %get-tuple-element.54), channel_id=1, source_target_pairs={{0,6},{1,7},{2,4},{3,5},{4,2},{5,3},{6,0},{7,1},{8,14},{9,15},{10,... | collective-permute-start | bytes 1376264 | tf_op jit(solution)/shard_map/ppermute | solution.py:18
  101.3 26.2 %collective-permute-start.24 = (bf16[896,256]{1,0:T(8,128)(2,1)}, bf16[896,256]{1,0:T(8,128)(2,1)S(1)}, u32[]{:S(2)}, u32[]{:S(2)}) collective-permute-start(bf16[896,256]{1,0:T(8,128)(2,1)} %get-tuple-element.55), channel_id=1, source_target_pairs={{0,7},{1,6},{2,5},{3,4},{4,3},{5,2},{6,1},{7,0},{8,15},{9,14},{10,... | collective-permute-start | bytes 1376264 | tf_op jit(solution)/shard_map/ppermute | solution.py:18
  102.3 26.1 %collective-permute-start.27 = (bf16[896,256]{1,0:T(8,128)(2,1)}, bf16[896,256]{1,0:T(8,128)(2,1)S(1)}, u32[]{:S(2)}, u32[]{:S(2)}) collective-permute-start(bf16[896,256]{1,0:T(8,128)(2,1)} %get-tuple-element.60), channel_id=1, source_target_pairs={{0,1},{1,0},{2,3},{3,2},{4,5},{5,4},{6,7},{7,6},{8,9},{9,8},{10,11... | collective-permute-start | bytes 1376264 | tf_op jit(solution)/shard_map/ppermute | solution.py:18
  124.1 11.3 %collective-permute-start.28 = (bf16[896,256]{1,0:T(8,128)(2,1)}, bf16[896,256]{1,0:T(8,128)(2,1)S(1)}, u32[]{:S(2)}, u32[]{:S(2)}) collective-permute-start(bf16[896,256]{1,0:T(8,128)(2,1)} %get-tuple-element.61), channel_id=1, source_target_pairs={{0,2},{1,3},{2,0},{3,1},{4,6},{5,7},{6,4},{7,5},{8,10},{9,11},{10,... | collective-permute-start | bytes 1376264 | tf_op jit(solution)/shard_map/ppermute | solution.py:18
  126.1 34.3 %collective-permute-start.29 = (bf16[896,256]{1,0:T(8,128)(2,1)}, bf16[896,256]{1,0:T(8,128)(2,1)S(1)}, u32[]{:S(2)}, u32[]{:S(2)}) collective-permute-start(bf16[896,256]{1,0:T(8,128)(2,1)} %get-tuple-element.62), channel_id=1, source_target_pairs={{0,3},{1,2},{2,1},{3,0},{4,7},{5,6},{6,5},{7,4},{8,11},{9,10},{10,... | collective-permute-start | bytes 1376264 | tf_op jit(solution)/shard_map/ppermute | solution.py:18
  127.5 32.9 %collective-permute-start.30 = (bf16[896,256]{1,0:T(8,128)(2,1)}, bf16[896,256]{1,0:T(8,128)(2,1)S(1)}, u32[]{:S(2)}, u32[]{:S(2)}) collective-permute-start(bf16[896,256]{1,0:T(8,128)(2,1)} %get-tuple-element.63), channel_id=1, source_target_pairs={{0,4},{1,5},{2,6},{3,7},{4,0},{5,1},{6,2},{7,3},{8,12},{9,13},{10,... | collective-permute-start | bytes 1376264 | tf_op jit(solution)/shard_map/ppermute | solution.py:18
  128.4 40.8 %collective-permute-start.31 = (bf16[896,256]{1,0:T(8,128)(2,1)}, bf16[896,256]{1,0:T(8,128)(2,1)S(1)}, u32[]{:S(2)}, u32[]{:S(2)}) collective-permute-start(bf16[896,256]{1,0:T(8,128)(2,1)} %get-tuple-element.64), channel_id=1, source_target_pairs={{0,5},{1,4},{2,7},{3,6},{4,1},{5,0},{6,3},{7,2},{8,13},{9,12},{10,... | collective-permute-start | bytes 1376264 | tf_op jit(solution)/shard_map/ppermute | solution.py:18
  135.4 38.5 %collective-permute-start.25 = (bf16[896,256]{1,0:T(8,128)(2,1)}, bf16[896,256]{1,0:T(8,128)(2,1)S(1)}, u32[]{:S(2)}, u32[]{:S(2)}) collective-permute-start(bf16[896,256]{1,0:T(8,128)(2,1)} %get-tuple-element.57), channel_id=1, source_target_pairs={{0,6},{1,7},{2,4},{3,5},{4,2},{5,3},{6,0},{7,1},{8,14},{9,15},{10,... | collective-permute-start | bytes 1376264 | tf_op jit(solution)/shard_map/ppermute | solution.py:18
  137.3 36.6 %collective-permute-start.26 = (bf16[896,256]{1,0:T(8,128)(2,1)}, bf16[896,256]{1,0:T(8,128)(2,1)S(1)}, u32[]{:S(2)}, u32[]{:S(2)}) collective-permute-start(bf16[896,256]{1,0:T(8,128)(2,1)} %get-tuple-element.58), channel_id=1, source_target_pairs={{0,7},{1,6},{2,5},{3,4},{4,3},{5,2},{6,1},{7,0},{8,15},{9,14},{10,... | collective-permute-start | bytes 1376264 | tf_op jit(solution)/shard_map/ppermute | solution.py:18
  160.5 20.6 %collective-permute-start.32 = (f32[4,2,64,256]{3,2,1,0:T(8,128)}, f32[4,2,64,256]{3,2,1,0:T(8,128)}, u32[]{:S(2)}, u32[]{:S(2)}) collective-permute-start(f32[4,2,64,256]{3,2,1,0:T(8,128)} %get-tuple-element.67), channel_id=1, source_target_pairs={{0,1},{1,0},{2,3},{3,2},{4,5},{5,4},{6,7},{7,6},{8,9},{9,8},{10,11... | collective-permute-start | bytes 1572872 | tf_op jit(solution)/shard_map/ppermute | solution.py:18
  173.2 21.5 %collective-permute-start.37 = (f32[4,4,64,256]{3,2,1,0:T(8,128)}, f32[4,4,64,256]{3,2,1,0:T(8,128)}, u32[]{:S(2)}, u32[]{:S(2)}) collective-permute-start(f32[4,4,64,256]{3,2,1,0:T(8,128)} %get-tuple-element.69), channel_id=1, source_target_pairs={{0,1},{1,0},{2,3},{3,2},{4,5},{5,4},{6,7},{7,6},{8,9},{9,8},{10,11... | collective-permute-start | bytes 3145736 | tf_op jit(solution)/shard_map/ppermute | solution.py:18
  187.2 10.7 %collective-permute-start.47 = (bf16[2,64,256]{2,1,0:T(8,128)(2,1)S(1)}, bf16[2,64,256]{2,1,0:T(8,128)(2,1)S(1)}, u32[]{:S(2)}, u32[]{:S(2)}) collective-permute-start(bf16[2,64,256]{2,1,0:T(8,128)(2,1)S(1)} %get-tuple-element.86), channel_id=1, source_target_pairs={{0,16},{8,24},{16,0},{24,8},{1,17},{9,25},{17,1},{25,9},{2,18},{10... | collective-permute-start | bytes 196616 | tf_op jit(solution)/shard_map/ppermute | solution.py:18
  190.8 25.0 %collective-permute-start.36 = (bf16[64,256]{1,0:T(8,128)(2,1)S(1)}, bf16[64,256]{1,0:T(8,128)(2,1)S(1)}, u32[]{:S(2)}, u32[]{:S(2)}) collective-permute-start(bf16[64,256]{1,0:T(8,128)(2,1)S(1)} %get-tuple-element.93), channel_id=1, source_target_pairs={{0,1},{1,0},{2,3},{3,2},{4,5},{5,4},{6,7},{7,6},{8,9},{9,8},{10,11... | collective-permute-start | bytes 98312 | tf_op jit(solution)/shard_map/ppermute | solution.py:18
  196.2 10.1 %collective-permute-start.39 = (bf16[4,64,256]{2,1,0:T(8,128)(2,1)S(1)}, bf16[4,64,256]{2,1,0:T(8,128)(2,1)S(1)}, u32[]{:S(2)}, u32[]{:S(2)}) collective-permute-start(bf16[4,64,256]{2,1,0:T(8,128)(2,1)S(1)} %get-tuple-element.78), channel_id=1, source_target_pairs={{0,16},{8,24},{16,0},{24,8},{1,17},{9,25},{17,1},{25,9},{2,18},{10... | collective-permute-start | bytes 393224 | tf_op jit(solution)/shard_map/ppermute | solution.py:18
  197.9 10.3 %collective-permute-start.40 = (bf16[4,64,256]{2,1,0:T(8,128)(2,1)S(1)}, bf16[4,64,256]{2,1,0:T(8,128)(2,1)S(1)}, u32[]{:S(2)}, u32[]{:S(2)}) collective-permute-start(bf16[4,64,256]{2,1,0:T(8,128)(2,1)S(1)} %get-tuple-element.77), channel_id=1, source_target_pairs={{0,24},{8,16},{16,8},{24,0},{1,25},{9,17},{17,9},{25,1},{2,26},{10... | collective-permute-start | bytes 393224 | tf_op jit(solution)/shard_map/ppermute | solution.py:18
  199.8 11.2 %collective-permute-start.49 = (bf16[64,256]{1,0:T(8,128)(2,1)S(1)}, bf16[64,256]{1,0:T(8,128)(2,1)S(1)}, u32[]{:S(2)}, u32[]{:S(2)}) collective-permute-start(bf16[64,256]{1,0:T(8,128)(2,1)S(1)} %get-tuple-element.102), channel_id=1, source_target_pairs={{0,6},{1,7},{2,4},{3,5},{4,2},{5,3},{6,0},{7,1},{8,14},{9,15},{10,... | collective-permute-start | bytes 98312 | tf_op jit(solution)/shard_map/ppermute | solution.py:18
  (56 other events, 416.5 us)
where the time goes:
time: 218 us; the launch traced here: 217 us
  waiting for transfers between devices  90.1 us (41%)
  starting transfers between devices  59.6 us (27%)
  Pallas kernels  47.3 us (22%)
  local copies, waits for them, and re-layouts  8.62 us (4%)
  other arithmetic  8.15 us (4%)
    ppermute x51, waiting for transfers between devices, swap(): return lax.ppermute(value, axis, pairs)  90.1 us
    ppermute x51, starting transfers between devices, swap(): return lax.ppermute(value, axis, pairs)  59.6 us
    pallas_call x4, Pallas kernels, ready(): pl.pallas_call(functools.partial(ready_kernel, masks), in_specs=in_specs,...  18.7 us
    pallas_call x2, Pallas kernels, slab_call(): pl.pallas_call(functools.partial(kernel, len(pieces)), grid_spec=pltpu.Pr...  13.3 us
    pallas_call x3, Pallas kernels, dots_call(): pl.pallas_call(functools.partial(dots_kernel, len(pieces)), in_specs=[pl....  9.75 us
    unnamed x75, local copies, waits for them, and re-layouts  7.58 us
  transfers between devices with their start and end apart: 51, of which 16 were waited for; matrix products, arithmetic and copies ran while one was open for 3% of the time, Pallas kernels for 21%

commit v1 on v0

--- a/solution.py
+++ b/solution.py
@@ -83,7 +83,7 @@
             pltpu.VMEM((count, rows, width), jnp.float32),
             pltpu.SemaphoreType.DMA((count,)),
         ],
-        compiler_params=pltpu.CompilerParams(vmem_limit_bytes=60 * 2**20),
+        compiler_params=pltpu.CompilerParams(vmem_limit_bytes=57 * 2**20),
         cost_estimate=pl.CostEstimate(
             flops=10**8, bytes_accessed=6 * count * rows * width, transcendentals=0
         ),
@@ -151,7 +151,7 @@
         out_shape=jax.ShapeDtypeStruct((1, rows, model), jnp.bfloat16),
         input_output_aliases={} if slab is None else {1 + count: 0},
         scratch_shapes=[pltpu.SemaphoreType.DMA((count,))],
-        compiler_params=pltpu.CompilerParams(vmem_limit_bytes=52 * 2**20),
+        compiler_params=pltpu.CompilerParams(vmem_limit_bytes=16 * 2**20),
         cost_estimate=pl.CostEstimate(
             flops=10**8, bytes_accessed=4 * count * rows * width, transcendentals=0
         ),
@@ -181,7 +181,7 @@
             out_specs=out_specs,
         ),
         out_shape=out_shape,
-        compiler_params=pltpu.CompilerParams(vmem_limit_bytes=52 * 2**20),
+        compiler_params=pltpu.CompilerParams(vmem_limit_bytes=24 * 2**20),
         cost_estimate=pl.CostEstimate(
             flops=2 * rows * block_rows * model + 10**8,
             bytes_accessed=4 * block_rows * model,
@@ -205,19 +205,20 @@
                 )
                 for t in range(tiles)
             )
-            target[:, slot] = out.reshape(blocks, rows, width)
+            target[:, slot] = out.reshape(blocks, rows, width).astype(target.dtype)
 
 
 def dots_call(hidden, pieces, blocks):
     rows = hidden.shape[1]
     inner, width = pieces[0].shape
-    out = jax.ShapeDtypeStruct((blocks, len(pieces), rows // 2 // blocks, width), jnp.float32)
+    shape = (blocks, len(pieces), rows // 2 // blocks, width)
+    outs = [jax.ShapeDtypeStruct(shape, kind) for kind in (jnp.bfloat16, jnp.float32)]
     return pl.pallas_call(
         functools.partial(dots_kernel, len(pieces)),
         in_specs=[pl.BlockSpec(memory_space=pltpu.VMEM)] * (1 + len(pieces)),
         out_specs=[pl.BlockSpec(memory_space=pltpu.VMEM)] * 2,
-        out_shape=[out, out],
-        compiler_params=pltpu.CompilerParams(vmem_limit_bytes=52 * 2**20),
+        out_shape=outs,
+        compiler_params=pltpu.CompilerParams(vmem_limit_bytes=16 * 2**20),
         cost_estimate=pl.CostEstimate(
             flops=2 * rows * inner * width * len(pieces) + 10**8,
             bytes_accessed=2 * inner * width * len(pieces),
@@ -269,6 +270,7 @@
         placed.reshape(experts * capacity, tok_rows), tokens, preferred_element_type=jnp.float32
     )
     picked = picked.astype(jnp.bfloat16).reshape(slabs, half_cap, tokens.shape[1])
+    picked, spread, share = lax.optimization_barrier((picked, spread, share))
     chunks = [
         swap(lax.dynamic_index_in_dim(picked, me ^ m, 0, keepdims=False), "tp", m)
         for m in range(slabs)
@@ -294,7 +296,7 @@
         masks = [mask for pair in group for mask in (2 * pair, 2 * pair + 1)]
         sent, own = dots_call(hidden, [down_pieces[m] for m in masks], blocks)
         got = swap(sent, "tp", 1)
-        parts = [(own[z] + got[z]).astype(jnp.bfloat16) for z in range(blocks)]
+        parts = [(own[z] + got[z].astype(jnp.float32)).astype(jnp.bfloat16) for z in range(blocks)]
         if direct:
             parts = [swap(part, "fs", z) for z, part in enumerate(parts)]
         else:
@@ -310,7 +312,7 @@
             down_serve = fill_call(me_ref, pieces, filled, model, down_serve)
 
     mixed = jnp.zeros((tok_rows, tokens.shape[1]), jnp.float32)
-    for pair in range(experts):
+    for pair in reversed(range(experts)):
         rows = jnp.concatenate([backs[2 * pair], backs[2 * pair + 1]])
         term = lax.dot_general(
             spread[pair], rows, (((0,), (0,)), ((), ())), preferred_element_type=jnp.float32

time: 218 us -> 224 us (1.028)
  waiting for transfers between devices: 90.1 us -> 123 us
  Pallas kernels: 47.3 us -> 33.7 us
  starting transfers between devices: 59.6 us -> 48.9 us
  other arithmetic: 8.15 us -> 4.94 us
    ppermute x51, waiting for transfers between devices: 90.1 us -> 123 us  [swap(): return lax.ppermute(value, axis, pairs)]
    ppermute x51, starting transfers between devices: 59.6 us -> 48.9 us  [swap(): return lax.ppermute(value, axis, pairs)]
    pallas_call x3, Pallas kernels: 9.75 us -> 2.63 us  [dots_call(): pl.pallas_call(functools.partial(dots_kernel, len(pieces)), in_specs=[pl....]
    pallas_call x2, Pallas kernels: 13.3 us -> 8.17 us  [slab_call(): pl.pallas_call(functools.partial(kernel, len(pieces)), grid_spec=pltpu.Pr...]
    convert_element_type x3, other arithmetic: 3.79 us -> 0.27 us  [local(): (own[z] + got[z].astype(jnp.float32)).astype(jnp.bfloat16)]
    unnamed x75 -> x61, local copies, waits for them, and re-layouts: 7.58 us -> 6.03 us
  transfers between devices with their start and end apart: 51 -> 51, of which waited for: 16 -> 18; matrix products, arithmetic and copies ran while one was open for 3% -> 1% of each run, Pallas kernels for 21% -> 14%
where the time goes in v1:
time: 224 us; the launch traced here: 221 us
  waiting for transfers between devices  123 us (55%)
  starting transfers between devices  48.9 us (22%)
  Pallas kernels  33.7 us (15%)
  local copies, waits for them, and re-layouts  7.64 us (3%)
  other arithmetic  4.94 us (2%)
    ppermute x51, waiting for transfers between devices, swap(): return lax.ppermute(value, axis, pairs)  123 us
    ppermute x51, starting transfers between devices, swap(): return lax.ppermute(value, axis, pairs)  48.9 us
    pallas_call x4, Pallas kernels, ready(): pl.pallas_call(functools.partial(ready_kernel, masks), in_specs=in_specs,...  18.7 us
    pallas_call x2, Pallas kernels, slab_call(): pl.pallas_call(functools.partial(kernel, len(pieces)), grid_spec=pltpu.Pr...  8.17 us
    unnamed x61, local copies, waits for them, and re-layouts  6.03 us
  transfers between devices with their start and end apart: 51, of which 18 were waited for; matrix products, arithmetic and copies ran while one was open for 1% of the time, Pallas kernels for 14%

profile of v1, /device:TPU:1, one launch (start us, length us, event | category | flops | bytes accessed | tf_op | source)
XLA Modules:
  0.0 220.8 jit_solution(5591557777651664366)
XLA Ops:
  7.1 3.6 %collective-permute-start.6 = (bf16[64,256]{1,0:T(8,128)(2,1)S(1)}, bf16[64,256]{1,0:T(8,128)(2,1)S(1)}, u32[]{:S(2)}, u32[]{:S(2)}) collective-permute-start(bf16[64,256]{1,0:T(8,128)(2,1)S(1)} %get-tuple-element.114), channel_id=1, source_target_pairs={{0,7},{1,6},{2,5},{3,4},{4,3},{5,2},{6,1},{7,0},{8,15},{9,14},{10,... | collective-permute-start | bytes 98312 | tf_op jit(solution)/shard_map/ppermute | solution.py:18
  12.4 1.7 collective-permute-start.2
  17.9 1.8 norm_rows.1
  19.6 3.3 %collective-permute-start.9 = (bf16[64,2048]{1,0:T(8,128)(2,1)}, bf16[64,2048]{1,0:T(8,128)(2,1)S(1)}, u32[]{:S(2)}, u32[]{:S(2)}) collective-permute-start(bf16[64,2048]{1,0:T(8,128)(2,1)} %norm_rows.1), channel_id=1, source_target_pairs={{0,24},{8,16},{16,8},{24,0},{1,25},{9,17},{17,9},{25,1},{2,26},{10... | collective-permute-start | bytes 786440 | tf_op jit(solution)/shard_map/ppermute | solution.py:18
  22.9 3.1 %shard_map.103 = (bf16[896,256]{1,0:T(8,128)(2,1)}, bf16[896,256]{1,0:T(8,128)(2,1)}) custom-call(s32[1]{0:T(128)} %bitcast.me_ref, f32[8,896,256]{2,1,0:T(8,128)} %master_ref.5, f32[1,256]{1,0:T(1,128)} %bitcast.144), custom_call_target="tpu_custom_call" | custom-call | flops 100000000 | bytes 2752512 | tf_op jit(solution)/shard_map/pallas_call | solution.py:77
  28.3 4.8 %shard_map.102 = (bf16[896,256]{1,0:T(8,128)(2,1)}, bf16[896,256]{1,0:T(8,128)(2,1)}, bf16[896,256]{1,0:T(8,128)(2,1)}, bf16[896,256]{1,0:T(8,128)(2,1)}, bf16[8...) custom-call(s32[1]{0:T(128)} %bitcast.me_ref, f32[8,896,256]{2,1,0:T(8,128)} %master_ref.5, f32[1,256]{1,0:T(1,128)} %bitcast.145), custom_call_target="tpu_custom_call" | custom-call | flops 100000000 | bytes 8257536 | tf_op jit(solution)/shard_map/pallas_call | solution.py:77
  34.7 13.6 %collective-permute-done.8 = bf16[64,2048]{1,0:T(8,128)(2,1)S(1)} collective-permute-done((bf16[64,2048]{1,0:T(8,128)(2,1)S(1)}, bf16[64,2048]{1,0:T(8,128)(2,1)S(1)}, u32[]{:S(2)}, u32[]{:S(2)}) %collective-permute-start.8) | collective-permute-done | bytes 262176 | tf_op jit(solution)/shard_map/ppermute | solution.py:18
  49.6 5.7 %shard_map.105 = (bf16[896,256]{1,0:T(8,128)(2,1)}, bf16[896,256]{1,0:T(8,128)(2,1)}, bf16[896,256]{1,0:T(8,128)(2,1)}, bf16[896,256]{1,0:T(8,128)(2,1)}, bf16[8...) custom-call(s32[1]{0:T(128)} %bitcast.me_ref, ...), custom_call_target="tpu_custom_call" | custom-call | flops 100000000 | bytes 11010048 | tf_op jit(solution)/shard_map/pallas_call | solution.py:77
  55.3 1.7 collective-permute-start.16
  58.5 3.1 %collective-permute-done.13.refs_3_ = bf16[896,256]{1,0:T(8,128)(2,1)S(1)} collective-permute-done((bf16[896,256]{1,0:T(8,128)(2,1)}, bf16[896,256]{1,0:T(8,128)(2,1)S(1)}, u32[]{:S(2)}, u32[]{:S(2)}) %collective-permute-start.13) | collective-permute-done | bytes 458784 | tf_op jit(solution)/shard_map/ppermute | solution.py:18
  61.6 20.1 %collective-permute-done.15.refs_5_ = bf16[896,256]{1,0:T(8,128)(2,1)S(1)} collective-permute-done((bf16[896,256]{1,0:T(8,128)(2,1)}, bf16[896,256]{1,0:T(8,128)(2,1)S(1)}, u32[]{:S(2)}, u32[]{:S(2)}) %collective-permute-start.15) | collective-permute-done | bytes 458784 | tf_op jit(solution)/shard_map/ppermute | solution.py:18
  85.5 2.1 collective-permute-start.22
  87.6 6.8 %collective-permute-done.19.refs_2_ = bf16[896,256]{1,0:T(8,128)(2,1)S(1)} collective-permute-done((bf16[896,256]{1,0:T(8,128)(2,1)S(1)}, bf16[896,256]{1,0:T(8,128)(2,1)S(1)}, u32[]{:S(2)}, u32[]{:S(2)}) %collective-permute-start.19) | collective-permute-done | bytes 458784 | tf_op jit(solution)/shard_map/ppermute | solution.py:18
  94.3 5.0 %shard_map.107 = (bf16[896,256]{1,0:T(8,128)(2,1)}, bf16[896,256]{1,0:T(8,128)(2,1)}, bf16[896,256]{1,0:T(8,128)(2,1)}, bf16[896,256]{1,0:T(8,128)(2,1)}, bf16[8...) custom-call(s32[1]{0:T(128)} %bitcast.me_ref, ...), custom_call_target="tpu_custom_call" | custom-call | flops 100000000 | bytes 11010048 | tf_op jit(solution)/shard_map/pallas_call | solution.py:77
  99.4 2.0 collective-permute-done.20.refs_3_
  101.4 1.5 collective-permute-start.24
  104.5 22.3 %collective-permute-done.22.refs_5_ = bf16[896,256]{1,0:T(8,128)(2,1)S(1)} collective-permute-done((bf16[896,256]{1,0:T(8,128)(2,1)}, bf16[896,256]{1,0:T(8,128)(2,1)S(1)}, u32[]{:S(2)}, u32[]{:S(2)}) %collective-permute-start.22) | collective-permute-done | bytes 458784 | tf_op jit(solution)/shard_map/ppermute | solution.py:18
  127.7 1.9 collective-permute-start.25
  129.6 1.5 collective-permute-start.26
  131.1 8.0 %collective-permute-done.28.refs_2_.refs_0_ = bf16[896,256]{1,0:T(8,128)(2,1)S(1)} collective-permute-done((bf16[896,256]{1,0:T(8,128)(2,1)}, bf16[896,256]{1,0:T(8,128)(2,1)S(1)}, u32[]{:S(2)}, u32[]{:S(2)}) %collective-permute-start.28) | collective-permute-done | bytes 458784 | tf_op jit(solution)/shard_map/ppermute | solution.py:18
  144.1 4.1 %shard_map.104 = (bf16[1,896,2048]{2,1,0:T(8,128)(2,1)}, f32[2,512,448]{2,1,0:T(8,128)S(1)}) custom-call(s32[1]{0:T(128)} %bitcast.me_ref, bf16[256,2048]{1,0:T(8,128)(2,1)S(1)} %pad_maximum_fusion.mine_ref, bf16[256,2048]{1,0:T(8,128)(2,1)S(1)} %collective-permute-done.10.theirs_ref, bf16[896,256]{1,0:T(8,128)(2,1)S(1)} %copy-done.4, ...), custom_call_target="tpu_custom_call" | custom-call | flops 1979048192 | bytes 7340032 | tf_op jit(solution)/shard_map/pallas_call | solution.py:175
  148.3 4.1 %shard_map.106 = (bf16[1,896,2048]{2,1,0:T(8,128)(2,1)}, bf16[2,512,448]{2,1,0:T(8,128)(2,1)S(1)}) custom-call(s32[1]{0:T(128)} %bitcast.me_ref, bf16[256,2048]{1,0:T(8,128)(2,1)S(1)} %pad_maximum_fusion.mine_ref, bf16[256,2048]{1,0:T(8,128)(2,1)S(1)} %collective-permute-done.10.theirs_ref, f32[2,512,448]{2,1,0:T(8,128)S(1)} %get-tuple-element.57.act_ref, ...), custom_call_target="tpu_custom_call" | custom-call | flops 1979048192 | bytes 7340032 | tf_op jit(solution)/shard_map/pallas_call | solution.py:175
  153.4 17.4 %collective-permute-done.30.refs_4_.refs_2_ = bf16[896,256]{1,0:T(8,128)(2,1)S(1)} collective-permute-done((bf16[896,256]{1,0:T(8,128)(2,1)}, bf16[896,256]{1,0:T(8,128)(2,1)S(1)}, u32[]{:S(2)}, u32[]{:S(2)}) %collective-permute-start.30) | collective-permute-done | bytes 458784 | tf_op jit(solution)/shard_map/ppermute | solution.py:18
  170.9 10.3 %collective-permute-done.31.refs_5_.refs_3_ = bf16[896,256]{1,0:T(8,128)(2,1)S(1)} collective-permute-done((bf16[896,256]{1,0:T(8,128)(2,1)}, bf16[896,256]{1,0:T(8,128)(2,1)S(1)}, u32[]{:S(2)}, u32[]{:S(2)}) %collective-permute-start.31) | collective-permute-done | bytes 458784 | tf_op jit(solution)/shard_map/ppermute | solution.py:18
  181.1 1.6 shard_map.108.refs_2_
  187.7 2.2 %collective-permute-start.47 = (bf16[2,64,256]{2,1,0:T(8,128)(2,1)S(1)}, bf16[2,64,256]{2,1,0:T(8,128)(2,1)S(1)}, u32[]{:S(2)}, u32[]{:S(2)}) collective-permute-start(bf16[2,64,256]{2,1,0:T(8,128)(2,1)S(1)} %get-tuple-element.105), channel_id=1, source_target_pairs={{0,8},{8,0},{16,24},{24,16},{1,9},{9,1},{17,25},{25,17},{2,10},{10... | collective-permute-start | bytes 196616 | tf_op jit(solution)/shard_map/ppermute | solution.py:18
  191.8 2.3 %collective-permute-done.48 = bf16[2,64,256]{2,1,0:T(8,128)(2,1)S(1)} collective-permute-done((bf16[2,64,256]{2,1,0:T(8,128)(2,1)S(1)}, bf16[2,64,256]{2,1,0:T(8,128)(2,1)S(1)}, u32[]{:S(2)}, u32[]{:S(2)}) %collective-permute-start.48) | collective-permute-done | bytes 65568 | tf_op jit(solution)/shard_map/ppermute | solution.py:18
  194.2 3.9 %collective-permute-start.50 = (bf16[64,256]{1,0:T(8,128)(2,1)S(1)}, bf16[64,256]{1,0:T(8,128)(2,1)S(1)}, u32[]{:S(2)}, u32[]{:S(2)}) collective-permute-start(bf16[64,256]{1,0:T(8,128)(2,1)S(1)} %get-tuple-element.113), channel_id=1, source_target_pairs={{0,1},{1,0},{2,3},{3,2},{4,5},{5,4},{6,7},{7,6},{8,9},{9,8},{10,11... | collective-permute-start | bytes 98312 | tf_op jit(solution)/shard_map/ppermute | solution.py:18
  198.4 2.9 %collective-permute-start.40 = (bf16[4,64,256]{2,1,0:T(8,128)(2,1)S(1)}, bf16[4,64,256]{2,1,0:T(8,128)(2,1)S(1)}, u32[]{:S(2)}, u32[]{:S(2)}) collective-permute-start(bf16[4,64,256]{2,1,0:T(8,128)(2,1)S(1)} %get-tuple-element.96), channel_id=1, source_target_pairs={{0,16},{8,24},{16,0},{24,8},{1,17},{9,25},{17,1},{25,9},{2,18},{10... | collective-permute-start | bytes 393224 | tf_op jit(solution)/shard_map/ppermute | solution.py:18
  202.1 3.2 %collective-permute-done.41 = bf16[4,64,256]{2,1,0:T(8,128)(2,1)S(1)} collective-permute-done((bf16[4,64,256]{2,1,0:T(8,128)(2,1)S(1)}, bf16[4,64,256]{2,1,0:T(8,128)(2,1)S(1)}, u32[]{:S(2)}, u32[]{:S(2)}) %collective-permute-start.41) | collective-permute-done | bytes 131104 | tf_op jit(solution)/shard_map/ppermute | solution.py:18
  205.5 7.9 %collective-permute-done.40 = bf16[4,64,256]{2,1,0:T(8,128)(2,1)S(1)} collective-permute-done((bf16[4,64,256]{2,1,0:T(8,128)(2,1)S(1)}, bf16[4,64,256]{2,1,0:T(8,128)(2,1)S(1)}, u32[]{:S(2)}, u32[]{:S(2)}) %collective-permute-start.40) | collective-permute-done | bytes 131104 | tf_op jit(solution)/shard_map/ppermute | solution.py:18
  213.9 2.1 collective-permute-start.43
  (180 shorter events, 44.1 us)
Async XLA Ops:
  19.6 14.8 %collective-permute-start.9 = (bf16[64,2048]{1,0:T(8,128)(2,1)}, bf16[64,2048]{1,0:T(8,128)(2,1)S(1)}, u32[]{:S(2)}, u32[]{:S(2)}) collective-permute-start(bf16[64,2048]{1,0:T(8,128)(2,1)} %norm_rows.1), channel_id=1, source_target_pairs={{0,24},{8,16},{16,8},{24,0},{1,25},{9,17},{17,9},{25,1},{2,26},{10... | collective-permute-start | bytes 786440 | tf_op jit(solution)/shard_map/ppermute | solution.py:18
  26.0 29.3 %collective-permute-start.12 = (bf16[896,256]{1,0:T(8,128)(2,1)}, bf16[896,256]{1,0:T(8,128)(2,1)S(1)}, u32[]{:S(2)}, u32[]{:S(2)}) collective-permute-start(bf16[896,256]{1,0:T(8,128)(2,1)} %get-tuple-element.50), channel_id=1, source_target_pairs={{0,2},{1,3},{2,0},{3,1},{4,6},{5,7},{6,4},{7,5},{8,10},{9,11},{10,... | collective-permute-start | bytes 1376264 | tf_op jit(solution)/shard_map/ppermute | solution.py:18
  27.0 30.0 %collective-permute-start.14 = (bf16[896,256]{1,0:T(8,128)(2,1)}, bf16[896,256]{1,0:T(8,128)(2,1)S(1)}, u32[]{:S(2)}, u32[]{:S(2)}) collective-permute-start(bf16[896,256]{1,0:T(8,128)(2,1)} %get-tuple-element.52), channel_id=1, source_target_pairs={{0,4},{1,5},{2,6},{3,7},{4,0},{5,1},{6,2},{7,3},{8,12},{9,13},{10,... | collective-permute-start | bytes 1376264 | tf_op jit(solution)/shard_map/ppermute | solution.py:18
  33.1 25.3 %collective-permute-start.11 = (bf16[896,256]{1,0:T(8,128)(2,1)}, bf16[896,256]{1,0:T(8,128)(2,1)S(1)}, u32[]{:S(2)}, u32[]{:S(2)}) collective-permute-start(bf16[896,256]{1,0:T(8,128)(2,1)} %get-tuple-element.49), channel_id=1, source_target_pairs={{0,1},{1,0},{2,3},{3,2},{4,5},{5,4},{6,7},{7,6},{8,9},{9,8},{10,11... | collective-permute-start | bytes 1376264 | tf_op jit(solution)/shard_map/ppermute | solution.py:18
  34.5 13.8 %collective-permute-start.8 = (bf16[64,2048]{1,0:T(8,128)(2,1)S(1)}, bf16[64,2048]{1,0:T(8,128)(2,1)S(1)}, u32[]{:S(2)}, u32[]{:S(2)}) collective-permute-start(bf16[64,2048]{1,0:T(8,128)(2,1)S(1)} %copy-done.11), channel_id=1, source_target_pairs={{0,16},{8,24},{16,0},{24,8},{1,17},{9,25},{17,1},{25,9},{2,18},{10... | collective-permute-start | bytes 786440 | tf_op jit(solution)/shard_map/ppermute | solution.py:18
  34.5 15.0 %collective-permute-start.7 = (bf16[64,2048]{1,0:T(8,128)(2,1)S(1)}, bf16[64,2048]{1,0:T(8,128)(2,1)S(1)}, u32[]{:S(2)}, u32[]{:S(2)}) collective-permute-start(bf16[64,2048]{1,0:T(8,128)(2,1)S(1)} %copy-done.11), channel_id=1, source_target_pairs={{0,8},{8,0},{16,24},{24,16},{1,9},{9,1},{17,25},{25,17},{2,10},{10... | collective-permute-start | bytes 786440 | tf_op jit(solution)/shard_map/ppermute | solution.py:18
  48.3 13.3 %collective-permute-start.13 = (bf16[896,256]{1,0:T(8,128)(2,1)}, bf16[896,256]{1,0:T(8,128)(2,1)S(1)}, u32[]{:S(2)}, u32[]{:S(2)}) collective-permute-start(bf16[896,256]{1,0:T(8,128)(2,1)} %get-tuple-element.51), channel_id=1, source_target_pairs={{0,3},{1,2},{2,1},{3,0},{4,7},{5,6},{6,5},{7,4},{8,11},{9,10},{10,... | collective-permute-start | bytes 1376264 | tf_op jit(solution)/shard_map/ppermute | solution.py:18
  49.4 32.3 %collective-permute-start.15 = (bf16[896,256]{1,0:T(8,128)(2,1)}, bf16[896,256]{1,0:T(8,128)(2,1)S(1)}, u32[]{:S(2)}, u32[]{:S(2)}) collective-permute-start(bf16[896,256]{1,0:T(8,128)(2,1)} %get-tuple-element.53), channel_id=1, source_target_pairs={{0,5},{1,4},{2,7},{3,6},{4,1},{5,0},{6,3},{7,2},{8,13},{9,12},{10,... | collective-permute-start | bytes 1376264 | tf_op jit(solution)/shard_map/ppermute | solution.py:18
  55.3 27.9 %collective-permute-start.16 = (bf16[896,256]{1,0:T(8,128)(2,1)S(1)}, bf16[896,256]{1,0:T(8,128)(2,1)S(1)}, u32[]{:S(2)}, u32[]{:S(2)}) collective-permute-start(bf16[896,256]{1,0:T(8,128)(2,1)S(1)} %copy-done.28), channel_id=1, source_target_pairs={{0,6},{1,7},{2,4},{3,5},{4,2},{5,3},{6,0},{7,1},{8,14},{9,15},{10,... | collective-permute-start | bytes 1376264 | tf_op jit(solution)/shard_map/ppermute | solution.py:18
  57.0 27.0 %collective-permute-start.17 = (bf16[896,256]{1,0:T(8,128)(2,1)S(1)}, bf16[896,256]{1,0:T(8,128)(2,1)S(1)}, u32[]{:S(2)}, u32[]{:S(2)}) collective-permute-start(bf16[896,256]{1,0:T(8,128)(2,1)S(1)} %copy-done.27), channel_id=1, source_target_pairs={{0,7},{1,6},{2,5},{3,4},{4,3},{5,2},{6,1},{7,0},{8,15},{9,14},{10,... | collective-permute-start | bytes 1376264 | tf_op jit(solution)/shard_map/ppermute | solution.py:18
  58.4 27.1 %collective-permute-start.18 = (bf16[896,256]{1,0:T(8,128)(2,1)}, bf16[896,256]{1,0:T(8,128)(2,1)S(1)}, u32[]{:S(2)}, u32[]{:S(2)}) collective-permute-start(bf16[896,256]{1,0:T(8,128)(2,1)} %get-tuple-element.59), channel_id=1, source_target_pairs={{0,1},{1,0},{2,3},{3,2},{4,5},{5,4},{6,7},{7,6},{8,9},{9,8},{10,11... | collective-permute-start | bytes 1376264 | tf_op jit(solution)/shard_map/ppermute | solution.py:18
  61.6 78.1 %collective-permute-start.10 = (bf16[256,2048]{1,0:T(8,128)(2,1)S(1)}, bf16[256,2048]{1,0:T(8,128)(2,1)S(1)}, u32[]{:S(2)}, u32[]{:S(2)}) collective-permute-start(bf16[256,2048]{1,0:T(8,128)(2,1)S(1)} %pad_maximum_fusion.mine_ref), channel_id=1, source_target_pairs={{0,1},{1,0},{2,3},{3,2},{4,5},{5,4},{6,7},{7,6},{8,9},{9,8},{10,11... | collective-permute-start | bytes 3145736 | tf_op jit(solution)/shard_map/ppermute | solution.py:18
  82.5 11.8 %collective-permute-start.19 = (bf16[896,256]{1,0:T(8,128)(2,1)S(1)}, bf16[896,256]{1,0:T(8,128)(2,1)S(1)}, u32[]{:S(2)}, u32[]{:S(2)}) collective-permute-start(bf16[896,256]{1,0:T(8,128)(2,1)S(1)} %copy-done.29), channel_id=1, source_target_pairs={{0,2},{1,3},{2,0},{3,1},{4,6},{5,7},{6,4},{7,5},{8,10},{9,11},{10,... | collective-permute-start | bytes 1376264 | tf_op jit(solution)/shard_map/ppermute | solution.py:18
  84.0 17.4 %collective-permute-start.20 = (bf16[896,256]{1,0:T(8,128)(2,1)}, bf16[896,256]{1,0:T(8,128)(2,1)S(1)}, u32[]{:S(2)}, u32[]{:S(2)}) collective-permute-start(bf16[896,256]{1,0:T(8,128)(2,1)} %get-tuple-element.61), channel_id=1, source_target_pairs={{0,3},{1,2},{2,1},{3,0},{4,7},{5,6},{6,5},{7,4},{8,11},{9,10},{10,... | collective-permute-start | bytes 1376264 | tf_op jit(solution)/shard_map/ppermute | solution.py:18
  84.8 18.2 %collective-permute-start.21 = (bf16[896,256]{1,0:T(8,128)(2,1)}, bf16[896,256]{1,0:T(8,128)(2,1)S(1)}, u32[]{:S(2)}, u32[]{:S(2)}) collective-permute-start(bf16[896,256]{1,0:T(8,128)(2,1)} %get-tuple-element.62), channel_id=1, source_target_pairs={{0,4},{1,5},{2,6},{3,7},{4,0},{5,1},{6,2},{7,3},{8,12},{9,13},{10,... | collective-permute-start | bytes 1376264 | tf_op jit(solution)/shard_map/ppermute | solution.py:18
  85.5 41.2 %collective-permute-start.22 = (bf16[896,256]{1,0:T(8,128)(2,1)}, bf16[896,256]{1,0:T(8,128)(2,1)S(1)}, u32[]{:S(2)}, u32[]{:S(2)}) collective-permute-start(bf16[896,256]{1,0:T(8,128)(2,1)} %get-tuple-element.63), channel_id=1, source_target_pairs={{0,5},{1,4},{2,7},{3,6},{4,1},{5,0},{6,3},{7,2},{8,13},{9,12},{10,... | collective-permute-start | bytes 1376264 | tf_op jit(solution)/shard_map/ppermute | solution.py:18
  94.3 33.2 %collective-permute-start.23 = (bf16[896,256]{1,0:T(8,128)(2,1)}, bf16[896,256]{1,0:T(8,128)(2,1)S(1)}, u32[]{:S(2)}, u32[]{:S(2)}) collective-permute-start(bf16[896,256]{1,0:T(8,128)(2,1)} %get-tuple-element.64), channel_id=1, source_target_pairs={{0,6},{1,7},{2,4},{3,5},{4,2},{5,3},{6,0},{7,1},{8,14},{9,15},{10,... | collective-permute-start | bytes 1376264 | tf_op jit(solution)/shard_map/ppermute | solution.py:18
  101.4 26.3 %collective-permute-start.24 = (bf16[896,256]{1,0:T(8,128)(2,1)}, bf16[896,256]{1,0:T(8,128)(2,1)S(1)}, u32[]{:S(2)}, u32[]{:S(2)}) collective-permute-start(bf16[896,256]{1,0:T(8,128)(2,1)} %get-tuple-element.65), channel_id=1, source_target_pairs={{0,7},{1,6},{2,5},{3,4},{4,3},{5,2},{6,1},{7,0},{8,15},{9,14},{10,... | collective-permute-start | bytes 1376264 | tf_op jit(solution)/shard_map/ppermute | solution.py:18
  103.0 26.6 %collective-permute-start.27 = (bf16[896,256]{1,0:T(8,128)(2,1)}, bf16[896,256]{1,0:T(8,128)(2,1)S(1)}, u32[]{:S(2)}, u32[]{:S(2)}) collective-permute-start(bf16[896,256]{1,0:T(8,128)(2,1)} %get-tuple-element.70), channel_id=1, source_target_pairs={{0,1},{1,0},{2,3},{3,2},{4,5},{5,4},{6,7},{7,6},{8,9},{9,8},{10,11... | collective-permute-start | bytes 1376264 | tf_op jit(solution)/shard_map/ppermute | solution.py:18
  126.7 12.5 %collective-permute-start.28 = (bf16[896,256]{1,0:T(8,128)(2,1)}, bf16[896,256]{1,0:T(8,128)(2,1)S(1)}, u32[]{:S(2)}, u32[]{:S(2)}) collective-permute-start(bf16[896,256]{1,0:T(8,128)(2,1)} %get-tuple-element.71), channel_id=1, source_target_pairs={{0,2},{1,3},{2,0},{3,1},{4,6},{5,7},{6,4},{7,5},{8,10},{9,11},{10,... | collective-permute-start | bytes 1376264 | tf_op jit(solution)/shard_map/ppermute | solution.py:18
  127.5 25.5 %collective-permute-start.29 = (bf16[896,256]{1,0:T(8,128)(2,1)}, bf16[896,256]{1,0:T(8,128)(2,1)S(1)}, u32[]{:S(2)}, u32[]{:S(2)}) collective-permute-start(bf16[896,256]{1,0:T(8,128)(2,1)} %get-tuple-element.72), channel_id=1, source_target_pairs={{0,3},{1,2},{2,1},{3,0},{4,7},{5,6},{6,5},{7,4},{8,11},{9,10},{10,... | collective-permute-start | bytes 1376264 | tf_op jit(solution)/shard_map/ppermute | solution.py:18
  127.7 55.0 %collective-permute-start.25 = (bf16[896,256]{1,0:T(8,128)(2,1)}, bf16[896,256]{1,0:T(8,128)(2,1)S(1)}, u32[]{:S(2)}, u32[]{:S(2)}) collective-permute-start(bf16[896,256]{1,0:T(8,128)(2,1)} %get-tuple-element.67), channel_id=1, source_target_pairs={{0,6},{1,7},{2,4},{3,5},{4,2},{5,3},{6,0},{7,1},{8,14},{9,15},{10,... | collective-permute-start | bytes 1376264 | tf_op jit(solution)/shard_map/ppermute | solution.py:18
  129.6 53.1 %collective-permute-start.26 = (bf16[896,256]{1,0:T(8,128)(2,1)}, bf16[896,256]{1,0:T(8,128)(2,1)S(1)}, u32[]{:S(2)}, u32[]{:S(2)}) collective-permute-start(bf16[896,256]{1,0:T(8,128)(2,1)} %get-tuple-element.68), channel_id=1, source_target_pairs={{0,7},{1,6},{2,5},{3,4},{4,3},{5,2},{6,1},{7,0},{8,15},{9,14},{10,... | collective-permute-start | bytes 1376264 | tf_op jit(solution)/shard_map/ppermute | solution.py:18
  139.2 31.7 %collective-permute-start.30 = (bf16[896,256]{1,0:T(8,128)(2,1)}, bf16[896,256]{1,0:T(8,128)(2,1)S(1)}, u32[]{:S(2)}, u32[]{:S(2)}) collective-permute-start(bf16[896,256]{1,0:T(8,128)(2,1)} %get-tuple-element.73), channel_id=1, source_target_pairs={{0,4},{1,5},{2,6},{3,7},{4,0},{5,1},{6,2},{7,3},{8,12},{9,13},{10,... | collective-permute-start | bytes 1376264 | tf_op jit(solution)/shard_map/ppermute | solution.py:18
  139.7 41.5 %collective-permute-start.31 = (bf16[896,256]{1,0:T(8,128)(2,1)}, bf16[896,256]{1,0:T(8,128)(2,1)S(1)}, u32[]{:S(2)}, u32[]{:S(2)}) collective-permute-start(bf16[896,256]{1,0:T(8,128)(2,1)} %get-tuple-element.74), channel_id=1, source_target_pairs={{0,5},{1,4},{2,7},{3,6},{4,1},{5,0},{6,3},{7,2},{8,13},{9,12},{10,... | collective-permute-start | bytes 1376264 | tf_op jit(solution)/shard_map/ppermute | solution.py:18
  153.0 33.2 %collective-permute-start.46 = (bf16[4,2,64,256]{3,2,1,0:T(8,128)(2,1)S(1)}, bf16[4,2,64,256]{3,2,1,0:T(8,128)(2,1)S(1)}, u32[]{:S(2)}, u32[]{:S(2)}) collective-permute-start(bf16[4,2,64,256]{3,2,1,0:T(8,128)(2,1)S(1)} %get-tuple-element.89), channel_id=1, source_target_pairs={{0,1},{1,0},{2,3},{3,2},{4,5},{5,4},{6,7},{7,6},{8,9},{9,8},{10,11... | collective-permute-start | bytes 786440 | tf_op jit(solution)/shard_map/ppermute | solution.py:18
  185.7 12.5 %collective-permute-start.38 = (bf16[4,4,64,256]{3,2,1,0:T(8,128)(2,1)S(1)}, bf16[4,4,64,256]{3,2,1,0:T(8,128)(2,1)S(1)}, u32[]{:S(2)}, u32[]{:S(2)}) collective-permute-start(bf16[4,4,64,256]{3,2,1,0:T(8,128)(2,1)S(1)} %get-tuple-element.83), channel_id=1, source_target_pairs={{0,1},{1,0},{2,3},{3,2},{4,5},{5,4},{6,7},{7,6},{8,9},{9,8},{10,11... | collective-permute-start | bytes 1572872 | tf_op jit(solution)/shard_map/ppermute | solution.py:18
  194.2 21.7 %collective-permute-start.50 = (bf16[64,256]{1,0:T(8,128)(2,1)S(1)}, bf16[64,256]{1,0:T(8,128)(2,1)S(1)}, u32[]{:S(2)}, u32[]{:S(2)}) collective-permute-start(bf16[64,256]{1,0:T(8,128)(2,1)S(1)} %get-tuple-element.113), channel_id=1, source_target_pairs={{0,1},{1,0},{2,3},{3,2},{4,5},{5,4},{6,7},{7,6},{8,9},{9,8},{10,11... | collective-permute-start | bytes 98312 | tf_op jit(solution)/shard_map/ppermute | solution.py:18
  198.4 14.9 %collective-permute-start.40 = (bf16[4,64,256]{2,1,0:T(8,128)(2,1)S(1)}, bf16[4,64,256]{2,1,0:T(8,128)(2,1)S(1)}, u32[]{:S(2)}, u32[]{:S(2)}) collective-permute-start(bf16[4,64,256]{2,1,0:T(8,128)(2,1)S(1)} %get-tuple-element.96), channel_id=1, source_target_pairs={{0,16},{8,24},{16,0},{24,8},{1,17},{9,25},{17,1},{25,9},{2,18},{10... | collective-permute-start | bytes 393224 | tf_op jit(solution)/shard_map/ppermute | solution.py:18
  201.3 12.0 %collective-permute-start.39 = (bf16[4,64,256]{2,1,0:T(8,128)(2,1)S(1)}, bf16[4,64,256]{2,1,0:T(8,128)(2,1)S(1)}, u32[]{:S(2)}, u32[]{:S(2)}) collective-permute-start(bf16[4,64,256]{2,1,0:T(8,128)(2,1)S(1)} %get-tuple-element.97), channel_id=1, source_target_pairs={{0,8},{8,0},{16,24},{24,16},{1,9},{9,1},{17,25},{25,17},{2,10},{10... | collective-permute-start | bytes 393224 | tf_op jit(solution)/shard_map/ppermute | solution.py:18
  202.0 17.9 %collective-permute-start.36 = (bf16[64,256]{1,0:T(8,128)(2,1)S(1)}, bf16[64,256]{1,0:T(8,128)(2,1)S(1)}, u32[]{:S(2)}, u32[]{:S(2)}) collective-permute-start(bf16[64,256]{1,0:T(8,128)(2,1)S(1)} %get-tuple-element.110), channel_id=1, source_target_pairs={{0,6},{1,7},{2,4},{3,5},{4,2},{5,3},{6,0},{7,1},{8,14},{9,15},{10,... | collective-permute-start | bytes 98312 | tf_op jit(solution)/shard_map/ppermute | solution.py:18
  205.3 14.7 %collective-permute-start.37 = (bf16[64,256]{1,0:T(8,128)(2,1)S(1)}, bf16[64,256]{1,0:T(8,128)(2,1)S(1)}, u32[]{:S(2)}, u32[]{:S(2)}) collective-permute-start(bf16[64,256]{1,0:T(8,128)(2,1)S(1)} %get-tuple-element.111), channel_id=1, source_target_pairs={{0,7},{1,6},{2,5},{3,4},{4,3},{5,2},{6,1},{7,0},{8,15},{9,14},{10,... | collective-permute-start | bytes 98312 | tf_op jit(solution)/shard_map/ppermute | solution.py:18
  (49 other events, 449.5 us)

commit v2 on v1

--- a/solution.py
+++ b/solution.py
@@ -190,41 +190,47 @@
     )(me, *wide, *(() if act is None else (act,)), *pieces)
 
 
-def dots_kernel(count, hidden_ref, *refs):
-    pieces, (sent_ref, own_ref) = refs[:count], refs[count:]
-    blocks, _, rows, width = own_ref.shape
-    half = blocks * rows
-    tiles, _, tile = hidden_ref.shape
-    for number, ref in enumerate(pieces):
-        for target, slot, start in ((sent_ref, number ^ 1, half), (own_ref, number, 0)):
-            out = sum(
+def dots_kernel(blocks, own_ref, other_ref, *refs):
+    outs = refs[-blocks:]
+    count = (len(refs) - blocks) // 2
+    tiles, rows, tile = own_ref.shape
+    half = rows // 2
+    for number in range(count):
+        own_piece, other_piece = refs[number], refs[count + number]
+        for side in range(2):
+            here, there = side * half, (1 - side) * half
+            total = sum(
                 jnp.dot(
-                    hidden_ref[t, start : start + half],
-                    ref[t * tile : (t + 1) * tile],
+                    hidden[t, start : start + half],
+                    piece[t * tile : (t + 1) * tile],
                     preferred_element_type=jnp.float32,
                 )
+                for hidden, start, piece in ((own_ref, here, own_piece), (other_ref, there, other_piece))
                 for t in range(tiles)
             )
-            target[:, slot] = out.reshape(blocks, rows, width).astype(target.dtype)
-
-
-def dots_call(hidden, pieces, blocks):
-    rows = hidden.shape[1]
-    inner, width = pieces[0].shape
-    shape = (blocks, len(pieces), rows // 2 // blocks, width)
-    outs = [jax.ShapeDtypeStruct(shape, kind) for kind in (jnp.bfloat16, jnp.float32)]
-    return pl.pallas_call(
-        functools.partial(dots_kernel, len(pieces)),
-        in_specs=[pl.BlockSpec(memory_space=pltpu.VMEM)] * (1 + len(pieces)),
-        out_specs=[pl.BlockSpec(memory_space=pltpu.VMEM)] * 2,
-        out_shape=outs,
+            total = total.astype(jnp.bfloat16).reshape(blocks, half // blocks, -1)
+            size = half // blocks
+            for z in range(blocks):
+                outs[z][number, side * size : (side + 1) * size] = total[z]
+
+
+def dots_call(own, other, own_pieces, other_pieces, blocks):
+    rows = own.shape[1]
+    inner, width = own_pieces[0].shape
+    count = len(own_pieces)
+    out = jax.ShapeDtypeStruct((count, rows // blocks, width), jnp.bfloat16)
+    return pl.pallas_call(
+        functools.partial(dots_kernel, blocks),
+        in_specs=[pl.BlockSpec(memory_space=pltpu.VMEM)] * (2 + 2 * count),
+        out_specs=[pl.BlockSpec(memory_space=pltpu.VMEM)] * blocks,
+        out_shape=[out] * blocks,
         compiler_params=pltpu.CompilerParams(vmem_limit_bytes=16 * 2**20),
         cost_estimate=pl.CostEstimate(
-            flops=2 * rows * inner * width * len(pieces) + 10**8,
-            bytes_accessed=2 * inner * width * len(pieces),
+            flops=4 * rows * inner * width * count + 10**8,
+            bytes_accessed=4 * inner * width * count,
             transcendentals=0,
         ),
-    )(hidden, *pieces)
+    )(own, other, *own_pieces, *other_pieces)
 
 
 def local(tokens, norm_gain, gate_master, up_master, down_master, routes, route_logits):
@@ -240,7 +246,13 @@
     def deliver(master, gain, groups):
         got = {}
         for masks in groups:
-            pieces = ready(master, gain, me_ref, masks)
+            if len(masks) > 2:
+                pieces = ready(master, gain, me_ref, masks)
+            else:
+                pieces = []
+                for mask in masks:
+                    piece = lax.dynamic_index_in_dim(master, me ^ mask, 0, keepdims=False)
+                    pieces.append((piece * gain[None, :]).astype(jnp.bfloat16))
             for mask, piece in zip(masks, pieces):
                 got[mask] = swap(piece, "tp", mask)
         return [got[mask] for mask in range(slabs)]
@@ -262,7 +274,12 @@
     placed = placed.astype(jnp.bfloat16)
     by_slab = placed.reshape(slabs, half_cap, tok_rows)
     spread = [
-        jnp.concatenate([lax.dynamic_index_in_dim(by_slab, me ^ m, 0, False) for m in (2 * p, 2 * p + 1)])
+        jnp.concatenate(
+            [
+                lax.dynamic_index_in_dim(by_slab, me ^ m, 0, False)
+                for m in ((2 * p + 1, 2 * p) if p else (0, 1))
+            ]
+        )
         for p in range(experts)
     ]
     share = [lax.dynamic_index_in_dim(weight, (me // 2) ^ p, 1) for p in range(experts)]
@@ -285,27 +302,32 @@
     theirs = swap(mine, "tp", 1)
 
     up_pieces = deliver(up_master, norm_gain, groups)
-    down_pieces = deliver(down_master, None, groups)
+    (masks,) = groups
+    made = dict(zip(masks, ready(down_master, None, me_ref, masks)))
+    down_pieces = [swap(made[mask], "tp", mask) for mask in range(slabs)]
 
     gate_serve, act = slab_call(gate_kernel, me_ref, (mine, theirs), None, gate_pieces, jnp.float32)
     up_serve, hidden = slab_call(up_kernel, me_ref, (mine, theirs), act, up_pieces, jnp.bfloat16)
+    other_hidden = swap(hidden, "tp", 1)
     backs = {}
     down_serve = None
-    pairs = pair_groups(experts)
-    for number, group in enumerate(pairs):
-        masks = [mask for pair in group for mask in (2 * pair, 2 * pair + 1)]
-        sent, own = dots_call(hidden, [down_pieces[m] for m in masks], blocks)
-        got = swap(sent, "tp", 1)
-        parts = [(own[z] + got[z].astype(jnp.float32)).astype(jnp.bfloat16) for z in range(blocks)]
+    for number, group in enumerate(pair_groups(experts)):
+        if number == 0:
+            own_pieces, other_pieces = [down_pieces[0]], [made[1]]
+        else:
+            own_pieces = [down_pieces[2 * pair + 1] for pair in group]
+            other_pieces = [swap(down_pieces[2 * pair], "tp", 1) for pair in group]
+        parts = dots_call(hidden, other_hidden, own_pieces, other_pieces, blocks)
         if direct:
             parts = [swap(part, "fs", z) for z, part in enumerate(parts)]
         else:
             parts = lax.all_to_all(jnp.stack(parts), "fs", split_axis=0, concat_axis=0, tiled=True)
-        for k, mask in enumerate(masks):
+        for k, pair in enumerate(group):
             total = sum(parts[z][k].astype(jnp.float32) for z in range(blocks))
             total = total.astype(jnp.bfloat16)
-            backs[mask] = swap(total, "tp", mask)
+            backs[pair] = swap(total, "tp", 2 * pair + 1) if pair else total
         if number > 0:
+            masks = [mask for pair in group for mask in (2 * pair, 2 * pair + 1)]
             filled = masks if number > 1 else [0, 1] + masks
             pieces = [down_pieces[m] for m in filled]
             model = down_pieces[0].shape[1] * slabs
@@ -313,9 +335,8 @@
 
     mixed = jnp.zeros((tok_rows, tokens.shape[1]), jnp.float32)
     for pair in reversed(range(experts)):
-        rows = jnp.concatenate([backs[2 * pair], backs[2 * pair + 1]])
         term = lax.dot_general(
-            spread[pair], rows, (((0,), (0,)), ((), ())), preferred_element_type=jnp.float32
+            spread[pair], backs[pair], (((0,), (0,)), ((), ())), preferred_element_type=jnp.float32
         )
         mixed = mixed + share[pair] * term
 

time: 224 us -> 226 us (level)
  waiting for transfers between devices: 123 us -> 80.4 us
  starting transfers between devices: 48.9 us -> 77.6 us
  local copies, waits for them, and re-layouts: 7.64 us -> 22.1 us
    ppermute x51 -> x48, waiting for transfers between devices: 123 us -> 80.4 us  [swap(): return lax.ppermute(value, axis, pairs)]
    ppermute x51 -> x48, starting transfers between devices: 48.9 us -> 77.6 us  [swap(): return lax.ppermute(value, axis, pairs)]
    unnamed x61 -> x77, local copies, waits for them, and re-layouts: 6.03 us -> 19.1 us
    pallas_call x4 -> x3, Pallas kernels: 18.7 us -> 15.6 us  [ready(): pl.pallas_call(functools.partial(ready_kernel, masks), in_specs=in_specs,...]
    pallas_call x2, Pallas kernels: 2.51 us -> 4.85 us  [fill_call(): pl.pallas_call(functools.partial(fill_kernel, masks), in_specs=in_specs,...]
  transfers between devices with their start and end apart: 51 -> 48, of which waited for: 18 -> 15; matrix products, arithmetic and copies ran while one was open for 1% -> 4% of each run, Pallas kernels for 14% -> 16%
where the time goes in v2:
time: 226 us; the launch traced here: 224 us
  waiting for transfers between devices  80.4 us (36%)
  starting transfers between devices  77.6 us (34%)
  Pallas kernels  35.2 us (16%)
  local copies, waits for them, and re-layouts  22.1 us (10%)
  other arithmetic  6.22 us (3%)
    ppermute x48, waiting for transfers between devices, swap(): return lax.ppermute(value, axis, pairs)  80.4 us
    ppermute x48, starting transfers between devices, swap(): return lax.ppermute(value, axis, pairs)  77.6 us
    unnamed x77, local copies, waits for them, and re-layouts  19.1 us
    pallas_call x3, Pallas kernels, ready(): pl.pallas_call(functools.partial(ready_kernel, masks), in_specs=in_specs,...  15.6 us
    pallas_call x2, Pallas kernels, slab_call(): pl.pallas_call(functools.partial(kernel, len(pieces)), grid_spec=pltpu.Pr...  8.17 us
    pallas_call x2, Pallas kernels, fill_call(): pl.pallas_call(functools.partial(fill_kernel, masks), in_specs=in_specs,...  4.85 us
    pallas_call x3, Pallas kernels, dots_call(): pl.pallas_call(functools.partial(dots_kernel, blocks), in_specs=[pl.Block...  4.83 us
  transfers between devices with their start and end apart: 48, of which 15 were waited for; matrix products, arithmetic and copies ran while one was open for 4% of the time, Pallas kernels for 16%

profile of v2, /device:TPU:1, one launch (start us, length us, event | category | flops | bytes accessed | tf_op | source)
XLA Modules:
  0.0 224.3 jit_solution(12430732258243781355)
XLA Ops:
  2.3 2.1 collective-permute-start.14
  10.2 2.0 collective-permute-start.6
  14.8 1.9 collective-permute-start.2
  21.8 3.3 %collective-permute-start.9 = (bf16[64,2048]{1,0:T(8,128)(2,1)}, bf16[64,2048]{1,0:T(8,128)(2,1)S(1)}, u32[]{:S(2)}, u32[]{:S(2)}) collective-permute-start(bf16[64,2048]{1,0:T(8,128)(2,1)} %norm_rows.1), channel_id=1, source_target_pairs={{0,24},{8,16},{16,8},{24,0},{1,25},{9,17},{17,9},{25,1},{2,26},{10... | collective-permute-start | bytes 786440 | tf_op jit(solution)/shard_map/ppermute | solution.py:18
  26.6 4.9 %shard_map.102 = (bf16[896,256]{1,0:T(8,128)(2,1)}, bf16[896,256]{1,0:T(8,128)(2,1)}, bf16[896,256]{1,0:T(8,128)(2,1)}, bf16[896,256]{1,0:T(8,128)(2,1)}, bf16[8...) custom-call(s32[1]{0:T(128)} %bitcast.me_ref, f32[8,896,256]{2,1,0:T(8,128)} %master_ref.3, f32[1,256]{1,0:T(1,128)} %bitcast.90), custom_call_target="tpu_custom_call" | custom-call | flops 100000000 | bytes 8257536 | tf_op jit(solution)/shard_map/pallas_call | solution.py:77
  31.5 3.1 %collective-permute-start.11 = (bf16[896,256]{1,0:T(8,128)(2,1)}, bf16[896,256]{1,0:T(8,128)(2,1)S(1)}, u32[]{:S(2)}, u32[]{:S(2)}) collective-permute-start(bf16[896,256]{1,0:T(8,128)(2,1)} %get-tuple-element.53), channel_id=1, source_target_pairs={{0,1},{1,0},{2,3},{3,2},{4,5},{5,4},{6,7},{7,6},{8,9},{9,8},{10,11... | collective-permute-start | bytes 1376264 | tf_op jit(solution)/shard_map/ppermute | solution.py:18
  34.6 12.7 %collective-permute-done.8 = bf16[64,2048]{1,0:T(8,128)(2,1)S(1)} collective-permute-done((bf16[64,2048]{1,0:T(8,128)(2,1)}, bf16[64,2048]{1,0:T(8,128)(2,1)S(1)}, u32[]{:S(2)}, u32[]{:S(2)}) %collective-permute-start.8) | collective-permute-done | bytes 262176 | tf_op jit(solution)/shard_map/ppermute | solution.py:18
  47.3 2.4 %collective-permute-start.13 = (bf16[896,256]{1,0:T(8,128)(2,1)}, bf16[896,256]{1,0:T(8,128)(2,1)S(1)}, u32[]{:S(2)}, u32[]{:S(2)}) collective-permute-start(bf16[896,256]{1,0:T(8,128)(2,1)} %get-tuple-element.54), channel_id=1, source_target_pairs={{0,3},{1,2},{2,1},{3,0},{4,7},{5,6},{6,5},{7,4},{8,11},{9,10},{10,... | collective-permute-start | bytes 1376264 | tf_op jit(solution)/shard_map/ppermute | solution.py:18
  52.0 1.8 collective-permute-start.17
  53.8 5.7 %shard_map.104 = (bf16[896,256]{1,0:T(8,128)(2,1)}, bf16[896,256]{1,0:T(8,128)(2,1)}, bf16[896,256]{1,0:T(8,128)(2,1)}, bf16[896,256]{1,0:T(8,128)(2,1)}, bf16[8...) custom-call(s32[1]{0:T(128)} %bitcast.me_ref, ...), custom_call_target="tpu_custom_call" | custom-call | flops 100000000 | bytes 11010048 | tf_op jit(solution)/shard_map/pallas_call | solution.py:77
  64.4 7.3 %collective-permute-done.16.refs_6_ = bf16[896,256]{1,0:T(8,128)(2,1)S(1)} collective-permute-done((bf16[896,256]{1,0:T(8,128)(2,1)}, bf16[896,256]{1,0:T(8,128)(2,1)S(1)}, u32[]{:S(2)}, u32[]{:S(2)}) %collective-permute-start.16) | collective-permute-done | bytes 458784 | tf_op jit(solution)/shard_map/ppermute | solution.py:18
  72.4 10.4 %collective-permute-start.20 = (bf16[896,256]{1,0:T(8,128)(2,1)}, bf16[896,256]{1,0:T(8,128)(2,1)S(1)}, u32[]{:S(2)}, u32[]{:S(2)}) collective-permute-start(bf16[896,256]{1,0:T(8,128)(2,1)} %get-tuple-element.63), channel_id=1, source_target_pairs={{0,3},{1,2},{2,1},{3,0},{4,7},{5,6},{6,5},{7,4},{8,11},{9,10},{10,... | collective-permute-start | bytes 1376264 | tf_op jit(solution)/shard_map/ppermute | solution.py:18
  83.6 1.8 collective-permute-start.21
  85.7 2.2 collective-permute-done.19.refs_2_
  87.9 8.2 %collective-permute-start.23 = (bf16[896,256]{1,0:T(8,128)(2,1)}, bf16[896,256]{1,0:T(8,128)(2,1)S(1)}, u32[]{:S(2)}, u32[]{:S(2)}) collective-permute-start(bf16[896,256]{1,0:T(8,128)(2,1)} %get-tuple-element.66), channel_id=1, source_target_pairs={{0,6},{1,7},{2,4},{3,5},{4,2},{5,3},{6,0},{7,1},{8,14},{9,15},{10,... | collective-permute-start | bytes 1376264 | tf_op jit(solution)/shard_map/ppermute | solution.py:18
  96.1 7.4 %collective-permute-done.20.refs_3_ = bf16[896,256]{1,0:T(8,128)(2,1)S(1)} collective-permute-done((bf16[896,256]{1,0:T(8,128)(2,1)}, bf16[896,256]{1,0:T(8,128)(2,1)S(1)}, u32[]{:S(2)}, u32[]{:S(2)}) %collective-permute-start.20) | collective-permute-done | bytes 458784 | tf_op jit(solution)/shard_map/ppermute | solution.py:18
  103.8 5.0 %shard_map.106 = (bf16[896,256]{1,0:T(8,128)(2,1)}, bf16[896,256]{1,0:T(8,128)(2,1)}, bf16[896,256]{1,0:T(8,128)(2,1)}, bf16[896,256]{1,0:T(8,128)(2,1)}, bf16[8...) custom-call(s32[1]{0:T(128)} %bitcast.me_ref, ...), custom_call_target="tpu_custom_call" | custom-call | flops 100000000 | bytes 11010048 | tf_op jit(solution)/shard_map/pallas_call | solution.py:77
  109.0 2.2 collective-permute-start.28
  117.3 4.1 %shard_map.103 = (bf16[1,896,2048]{2,1,0:T(8,128)(2,1)}, f32[2,512,448]{2,1,0:T(8,128)S(1)}) custom-call(s32[1]{0:T(128)} %bitcast.me_ref, bf16[256,2048]{1,0:T(8,128)(2,1)S(1)} %pad_maximum_fusion.mine_ref, bf16[256,2048]{1,0:T(8,128)(2,1)S(1)} %collective-permute-done.10.theirs_ref, bf16[896,256]{1,0:T(8,128)(2,1)S(1)} %copy-done.16, ...), custom_call_target="tpu_custom_call" | custom-call | flops 1979048192 | bytes 7340032 | tf_op jit(solution)/shard_map/pallas_call | solution.py:175
  121.4 14.7 %collective-permute-done.22.refs_5_ = bf16[896,256]{1,0:T(8,128)(2,1)S(1)} collective-permute-done((bf16[896,256]{1,0:T(8,128)(2,1)}, bf16[896,256]{1,0:T(8,128)(2,1)S(1)}, u32[]{:S(2)}, u32[]{:S(2)}) %collective-permute-start.22) | collective-permute-done | bytes 458784 | tf_op jit(solution)/shard_map/ppermute | solution.py:18
  142.5 4.0 %shard_map.105 = (bf16[1,896,2048]{2,1,0:T(8,128)(2,1)}, bf16[2,512,448]{2,1,0:T(8,128)(2,1)S(1)}) custom-call(s32[1]{0:T(128)} %bitcast.me_ref, bf16[256,2048]{1,0:T(8,128)(2,1)S(1)} %pad_maximum_fusion.mine_ref, bf16[256,2048]{1,0:T(8,128)(2,1)S(1)} %collective-permute-done.10.theirs_ref, f32[2,512,448]{2,1,0:T(8,128)S(1)} %get-tuple-element.59.act_ref, ...), custom_call_target="tpu_custom_call" | custom-call | flops 1979048192 | bytes 7340032 | tf_op jit(solution)/shard_map/pallas_call | solution.py:175
  151.3 18.8 %collective-permute-done.30.refs_4_ = bf16[896,256]{1,0:T(8,128)(2,1)} collective-permute-done((bf16[896,256]{1,0:T(8,128)(2,1)}, bf16[896,256]{1,0:T(8,128)(2,1)}, u32[]{:S(2)}, u32[]{:S(2)}) %collective-permute-start.30) | collective-permute-done | bytes 458784 | tf_op jit(solution)/shard_map/ppermute | solution.py:18
  171.6 8.5 %collective-permute-done.31.refs_5_.refs_1_ = bf16[896,256]{1,0:T(8,128)(2,1)S(1)} collective-permute-done((bf16[896,256]{1,0:T(8,128)(2,1)}, bf16[896,256]{1,0:T(8,128)(2,1)S(1)}, u32[]{:S(2)}, u32[]{:S(2)}) %collective-permute-start.31) | collective-permute-done | bytes 458784 | tf_op jit(solution)/shard_map/ppermute | solution.py:18
  180.6 2.7 %shard_map.107.refs_2_ = bf16[1,896,2048]{2,1,0:T(8,128)(2,1)} custom-call(s32[1]{0:T(128)} %bitcast.me_ref, bf16[896,256]{1,0:T(8,128)(2,1)S(1)} %copy-done.2, bf16[896,256]{1,0:T(8,128)(2,1)S(1)} %collective-permute-done.27.refs_1_, bf16[896,256]{1,0:T(8,128)(2,1)} %collective-permute-done.28.refs_2_, ...), custom_call_target="tpu_custom_call" | custom-call | flops 100000000 | bytes 5505024 | tf_op jit(solution)/shard_map/pallas_call | solution.py:147
  184.1 2.1 shard_map.108
  189.5 2.5 %collective-permute-start.46 = (bf16[1,128,256]{2,1,0:T(8,128)(2,1)S(1)}, bf16[1,128,256]{2,1,0:T(8,128)(2,1)S(1)}, u32[]{:S(2)}, u32[]{:S(2)}) collective-permute-start(bf16[1,128,256]{2,1,0:T(8,128)(2,1)S(1)} %get-tuple-element.96), channel_id=1, source_target_pairs={{0,16},{8,24},{16,0},{24,8},{1,17},{9,25},{17,1},{25,9},{2,18},{10... | collective-permute-start | bytes 196616 | tf_op jit(solution)/shard_map/ppermute | solution.py:18
  196.2 2.2 collective-permute-start.36
  199.4 2.4 %shard_map.110 = (bf16[2,128,256]{2,1,0:T(8,128)(2,1)S(1)}, bf16[2,128,256]{2,1,0:T(8,128)(2,1)S(1)}, bf16[2,128,256]{2,1,0:T(8,128)(2,1)S(1)}, bf16[2,128,256]{2,1,0:T(8,128)(2,1)S(1)}) custom-call(bf16[2,512,448]{2,1,0:T(8,128)(2,1)S(1)} %get-tuple-element.79.own_ref, bf16[2,512,448]{2,1,0:T(8,128)(2,1)S(1)} %copy.31.other_ref, ...), custom_call_target="tpu_custom_call" | custom-call | flops 1039524096 | bytes 1835008 | tf_op jit(solution)/shard_map/pallas_call | solution.py:222
  203.2 2.2 collective-permute-start.42
  205.5 2.2 collective-permute-done.40
  208.7 9.9 %collective-permute-start.37 = (bf16[128,256]{1,0:T(8,128)(2,1)S(1)}, bf16[128,256]{1,0:T(8,128)(2,1)S(1)}, u32[]{:S(2)}, u32[]{:S(2)}) collective-permute-start(bf16[128,256]{1,0:T(8,128)(2,1)S(1)} %fusion.7), channel_id=1, source_target_pairs={{0,7},{1,6},{2,5},{3,4},{4,3},{5,2},{6,1},{7,0},{8,15},{9,14},{10,... | collective-permute-start | bytes 196616 | tf_op jit(solution)/shard_map/ppermute | solution.py:18
  220.8 2.0 collective-permute-done.44
  (188 shorter events, 60.4 us)
Async XLA Ops:
  2.3 47.4 %collective-permute-start.14 = (bf16[896,256]{1,0:T(8,128)(2,1)S(1)}, bf16[896,256]{1,0:T(8,128)(2,1)S(1)}, u32[]{:S(2)}, u32[]{:S(2)}) collective-permute-start(bf16[896,256]{1,0:T(8,128)(2,1)S(1)} %get-tuple-element.102), channel_id=1, source_target_pairs={{0,4},{1,5},{2,6},{3,7},{4,0},{5,1},{6,2},{7,3},{8,12},{9,13},{10,... | collective-permute-start | bytes 1376264 | tf_op jit(solution)/shard_map/ppermute | solution.py:18
  25.2 22.1 %collective-permute-start.8 = (bf16[64,2048]{1,0:T(8,128)(2,1)}, bf16[64,2048]{1,0:T(8,128)(2,1)S(1)}, u32[]{:S(2)}, u32[]{:S(2)}) collective-permute-start(bf16[64,2048]{1,0:T(8,128)(2,1)} %norm_rows.1), channel_id=1, source_target_pairs={{0,16},{8,24},{16,0},{24,8},{1,17},{9,25},{17,1},{25,9},{2,18},{10... | collective-permute-start | bytes 786440 | tf_op jit(solution)/shard_map/ppermute | solution.py:18
  25.2 24.5 %collective-permute-start.7 = (bf16[64,2048]{1,0:T(8,128)(2,1)}, bf16[64,2048]{1,0:T(8,128)(2,1)S(1)}, u32[]{:S(2)}, u32[]{:S(2)}) collective-permute-start(bf16[64,2048]{1,0:T(8,128)(2,1)} %norm_rows.1), channel_id=1, source_target_pairs={{0,8},{8,0},{16,24},{24,16},{1,9},{9,1},{17,25},{25,17},{2,10},{10... | collective-permute-start | bytes 786440 | tf_op jit(solution)/shard_map/ppermute | solution.py:18
  25.4 25.5 %collective-permute-start.12 = (bf16[896,256]{1,0:T(8,128)(2,1)S(1)}, bf16[896,256]{1,0:T(8,128)(2,1)S(1)}, u32[]{:S(2)}, u32[]{:S(2)}) collective-permute-start(bf16[896,256]{1,0:T(8,128)(2,1)S(1)} %get-tuple-element.103), channel_id=1, source_target_pairs={{0,2},{1,3},{2,0},{3,1},{4,6},{5,7},{6,4},{7,5},{8,10},{9,11},{10,... | collective-permute-start | bytes 1376264 | tf_op jit(solution)/shard_map/ppermute | solution.py:18
  31.5 20.6 %collective-permute-start.11 = (bf16[896,256]{1,0:T(8,128)(2,1)}, bf16[896,256]{1,0:T(8,128)(2,1)S(1)}, u32[]{:S(2)}, u32[]{:S(2)}) collective-permute-start(bf16[896,256]{1,0:T(8,128)(2,1)} %get-tuple-element.53), channel_id=1, source_target_pairs={{0,1},{1,0},{2,3},{3,2},{4,5},{5,4},{6,7},{7,6},{8,9},{9,8},{10,11... | collective-permute-start | bytes 1376264 | tf_op jit(solution)/shard_map/ppermute | solution.py:18
  47.3 13.9 %collective-permute-start.13 = (bf16[896,256]{1,0:T(8,128)(2,1)}, bf16[896,256]{1,0:T(8,128)(2,1)S(1)}, u32[]{:S(2)}, u32[]{:S(2)}) collective-permute-start(bf16[896,256]{1,0:T(8,128)(2,1)} %get-tuple-element.54), channel_id=1, source_target_pairs={{0,3},{1,2},{2,1},{3,0},{4,7},{5,6},{6,5},{7,4},{8,11},{9,10},{10,... | collective-permute-start | bytes 1376264 | tf_op jit(solution)/shard_map/ppermute | solution.py:18
  49.7 12.8 %collective-permute-start.15 = (bf16[896,256]{1,0:T(8,128)(2,1)}, bf16[896,256]{1,0:T(8,128)(2,1)S(1)}, u32[]{:S(2)}, u32[]{:S(2)}) collective-permute-start(bf16[896,256]{1,0:T(8,128)(2,1)} %get-tuple-element.55), channel_id=1, source_target_pairs={{0,5},{1,4},{2,7},{3,6},{4,1},{5,0},{6,3},{7,2},{8,13},{9,12},{10,... | collective-permute-start | bytes 1376264 | tf_op jit(solution)/shard_map/ppermute | solution.py:18
  49.7 21.9 %collective-permute-start.16 = (bf16[896,256]{1,0:T(8,128)(2,1)}, bf16[896,256]{1,0:T(8,128)(2,1)S(1)}, u32[]{:S(2)}, u32[]{:S(2)}) collective-permute-start(bf16[896,256]{1,0:T(8,128)(2,1)} %get-tuple-element.56), channel_id=1, source_target_pairs={{0,6},{1,7},{2,4},{3,5},{4,2},{5,3},{6,0},{7,1},{8,14},{9,15},{10,... | collective-permute-start | bytes 1376264 | tf_op jit(solution)/shard_map/ppermute | solution.py:18
  51.0 58.0 %collective-permute-start.10 = (bf16[256,2048]{1,0:T(8,128)(2,1)S(1)}, bf16[256,2048]{1,0:T(8,128)(2,1)S(1)}, u32[]{:S(2)}, u32[]{:S(2)}) collective-permute-start(bf16[256,2048]{1,0:T(8,128)(2,1)S(1)} %pad_maximum_fusion.mine_ref), channel_id=1, source_target_pairs={{0,1},{1,0},{2,3},{3,2},{4,5},{5,4},{6,7},{7,6},{8,9},{9,8},{10,11... | collective-permute-start | bytes 3145736 | tf_op jit(solution)/shard_map/ppermute | solution.py:18
  52.0 30.8 %collective-permute-start.17 = (bf16[896,256]{1,0:T(8,128)(2,1)}, bf16[896,256]{1,0:T(8,128)(2,1)S(1)}, u32[]{:S(2)}, u32[]{:S(2)}) collective-permute-start(bf16[896,256]{1,0:T(8,128)(2,1)} %get-tuple-element.57), channel_id=1, source_target_pairs={{0,7},{1,6},{2,5},{3,4},{4,3},{5,2},{6,1},{7,0},{8,15},{9,14},{10,... | collective-permute-start | bytes 1376264 | tf_op jit(solution)/shard_map/ppermute | solution.py:18
  62.0 23.4 %collective-permute-start.18 = (bf16[896,256]{1,0:T(8,128)(2,1)}, bf16[896,256]{1,0:T(8,128)(2,1)S(1)}, u32[]{:S(2)}, u32[]{:S(2)}) collective-permute-start(bf16[896,256]{1,0:T(8,128)(2,1)} %get-tuple-element.61), channel_id=1, source_target_pairs={{0,1},{1,0},{2,3},{3,2},{4,5},{5,4},{6,7},{7,6},{8,9},{9,8},{10,11... | collective-permute-start | bytes 1376264 | tf_op jit(solution)/shard_map/ppermute | solution.py:18
  63.2 24.7 %collective-permute-start.19 = (bf16[896,256]{1,0:T(8,128)(2,1)}, bf16[896,256]{1,0:T(8,128)(2,1)S(1)}, u32[]{:S(2)}, u32[]{:S(2)}) collective-permute-start(bf16[896,256]{1,0:T(8,128)(2,1)} %get-tuple-element.62), channel_id=1, source_target_pairs={{0,2},{1,3},{2,0},{3,1},{4,6},{5,7},{6,4},{7,5},{8,10},{9,11},{10,... | collective-permute-start | bytes 1376264 | tf_op jit(solution)/shard_map/ppermute | solution.py:18
  72.4 31.0 %collective-permute-start.20 = (bf16[896,256]{1,0:T(8,128)(2,1)}, bf16[896,256]{1,0:T(8,128)(2,1)S(1)}, u32[]{:S(2)}, u32[]{:S(2)}) collective-permute-start(bf16[896,256]{1,0:T(8,128)(2,1)} %get-tuple-element.63), channel_id=1, source_target_pairs={{0,3},{1,2},{2,1},{3,0},{4,7},{5,6},{6,5},{7,4},{8,11},{9,10},{10,... | collective-permute-start | bytes 1376264 | tf_op jit(solution)/shard_map/ppermute | solution.py:18
  83.6 25.2 %collective-permute-start.21 = (bf16[896,256]{1,0:T(8,128)(2,1)}, bf16[896,256]{1,0:T(8,128)(2,1)S(1)}, u32[]{:S(2)}, u32[]{:S(2)}) collective-permute-start(bf16[896,256]{1,0:T(8,128)(2,1)} %get-tuple-element.64), channel_id=1, source_target_pairs={{0,4},{1,5},{2,6},{3,7},{4,0},{5,1},{6,2},{7,3},{8,12},{9,13},{10,... | collective-permute-start | bytes 1376264 | tf_op jit(solution)/shard_map/ppermute | solution.py:18
  85.4 50.7 %collective-permute-start.22 = (bf16[896,256]{1,0:T(8,128)(2,1)}, bf16[896,256]{1,0:T(8,128)(2,1)S(1)}, u32[]{:S(2)}, u32[]{:S(2)}) collective-permute-start(bf16[896,256]{1,0:T(8,128)(2,1)} %get-tuple-element.65), channel_id=1, source_target_pairs={{0,5},{1,4},{2,7},{3,6},{4,1},{5,0},{6,3},{7,2},{8,13},{9,12},{10,... | collective-permute-start | bytes 1376264 | tf_op jit(solution)/shard_map/ppermute | solution.py:18
  87.9 50.0 %collective-permute-start.23 = (bf16[896,256]{1,0:T(8,128)(2,1)}, bf16[896,256]{1,0:T(8,128)(2,1)S(1)}, u32[]{:S(2)}, u32[]{:S(2)}) collective-permute-start(bf16[896,256]{1,0:T(8,128)(2,1)} %get-tuple-element.66), channel_id=1, source_target_pairs={{0,6},{1,7},{2,4},{3,5},{4,2},{5,3},{6,0},{7,1},{8,14},{9,15},{10,... | collective-permute-start | bytes 1376264 | tf_op jit(solution)/shard_map/ppermute | solution.py:18
  103.4 35.2 %collective-permute-start.24 = (bf16[896,256]{1,0:T(8,128)(2,1)}, bf16[896,256]{1,0:T(8,128)(2,1)S(1)}, u32[]{:S(2)}, u32[]{:S(2)}) collective-permute-start(bf16[896,256]{1,0:T(8,128)(2,1)} %get-tuple-element.67), channel_id=1, source_target_pairs={{0,7},{1,6},{2,5},{3,4},{4,3},{5,2},{6,1},{7,0},{8,15},{9,14},{10,... | collective-permute-start | bytes 1376264 | tf_op jit(solution)/shard_map/ppermute | solution.py:18
  108.8 39.2 %collective-permute-start.25 = (bf16[896,256]{1,0:T(8,128)(2,1)}, bf16[896,256]{1,0:T(8,128)(2,1)}, u32[]{:S(2)}, u32[]{:S(2)}) collective-permute-start(bf16[896,256]{1,0:T(8,128)(2,1)} %get-tuple-element.69), channel_id=1, source_target_pairs={{0,6},{1,7},{2,4},{3,5},{4,2},{5,3},{6,0},{7,1},{8,14},{9,15},{10,... | collective-permute-start | bytes 1376264 | tf_op jit(solution)/shard_map/ppermute | solution.py:18
  109.0 40.7 %collective-permute-start.28 = (bf16[896,256]{1,0:T(8,128)(2,1)}, bf16[896,256]{1,0:T(8,128)(2,1)}, u32[]{:S(2)}, u32[]{:S(2)}) collective-permute-start(bf16[896,256]{1,0:T(8,128)(2,1)} %get-tuple-element.73), channel_id=1, source_target_pairs={{0,2},{1,3},{2,0},{3,1},{4,6},{5,7},{6,4},{7,5},{8,10},{9,11},{10,... | collective-permute-start | bytes 1376264 | tf_op jit(solution)/shard_map/ppermute | solution.py:18
  136.9 12.9 %collective-permute-start.29 = (bf16[896,256]{1,0:T(8,128)(2,1)}, bf16[896,256]{1,0:T(8,128)(2,1)S(1)}, u32[]{:S(2)}, u32[]{:S(2)}) collective-permute-start(bf16[896,256]{1,0:T(8,128)(2,1)} %get-tuple-element.74), channel_id=1, source_target_pairs={{0,3},{1,2},{2,1},{3,0},{4,7},{5,6},{6,5},{7,4},{8,11},{9,10},{10,... | collective-permute-start | bytes 1376264 | tf_op jit(solution)/shard_map/ppermute | solution.py:18
  147.0 39.2 %collective-permute-start.32 = (bf16[2,512,448]{1,2,0:T(8,128)(2,1)S(1)}, bf16[2,512,448]{1,2,0:T(8,128)(2,1)}, u32[]{:S(2)}, u32[]{:S(2)}) collective-permute-start(bf16[2,512,448]{1,2,0:T(8,128)(2,1)S(1)} %copy.30), channel_id=1, source_target_pairs={{0,1},{1,0},{2,3},{3,2},{4,5},{5,4},{6,7},{7,6},{8,9},{9,8},{10,11... | collective-permute-start | bytes 2752520 | tf_op jit(solution)/shard_map/ppermute | solution.py:18
  147.9 22.1 %collective-permute-start.30 = (bf16[896,256]{1,0:T(8,128)(2,1)}, bf16[896,256]{1,0:T(8,128)(2,1)}, u32[]{:S(2)}, u32[]{:S(2)}) collective-permute-start(bf16[896,256]{1,0:T(8,128)(2,1)} %get-tuple-element.75), channel_id=1, source_target_pairs={{0,4},{1,5},{2,6},{3,7},{4,0},{5,1},{6,2},{7,3},{8,12},{9,13},{10,... | collective-permute-start | bytes 1376264 | tf_op jit(solution)/shard_map/ppermute | solution.py:18
  148.0 32.1 %collective-permute-start.31 = (bf16[896,256]{1,0:T(8,128)(2,1)}, bf16[896,256]{1,0:T(8,128)(2,1)S(1)}, u32[]{:S(2)}, u32[]{:S(2)}) collective-permute-start(bf16[896,256]{1,0:T(8,128)(2,1)} %get-tuple-element.76), channel_id=1, source_target_pairs={{0,5},{1,4},{2,7},{3,6},{4,1},{5,0},{6,3},{7,2},{8,13},{9,12},{10,... | collective-permute-start | bytes 1376264 | tf_op jit(solution)/shard_map/ppermute | solution.py:18
  149.7 30.5 %collective-permute-start.27 = (bf16[896,256]{1,0:T(8,128)(2,1)S(1)}, bf16[896,256]{1,0:T(8,128)(2,1)S(1)}, u32[]{:S(2)}, u32[]{:S(2)}) collective-permute-start(bf16[896,256]{1,0:T(8,128)(2,1)S(1)} %copy-done.7), channel_id=1, source_target_pairs={{0,1},{1,0},{2,3},{3,2},{4,5},{5,4},{6,7},{7,6},{8,9},{9,8},{10,11... | collective-permute-start | bytes 1376264 | tf_op jit(solution)/shard_map/ppermute | solution.py:18
  149.8 34.3 %collective-permute-start.26 = (bf16[896,256]{1,0:T(8,128)(2,1)}, bf16[896,256]{1,0:T(8,128)(2,1)S(1)}, u32[]{:S(2)}, u32[]{:S(2)}) collective-permute-start(bf16[896,256]{1,0:T(8,128)(2,1)} %get-tuple-element.70), channel_id=1, source_target_pairs={{0,7},{1,6},{2,5},{3,4},{4,3},{5,2},{6,1},{7,0},{8,15},{9,14},{10,... | collective-permute-start | bytes 1376264 | tf_op jit(solution)/shard_map/ppermute | solution.py:18
  170.1 21.9 %collective-permute-start.33 = (bf16[896,256]{1,0:T(8,128)(2,1)}, bf16[896,256]{1,0:T(8,128)(2,1)}, u32[]{:S(2)}, u32[]{:S(2)}) collective-permute-start(bf16[896,256]{1,0:T(8,128)(2,1)} %collective-permute-done.25.refs_0_), channel_id=1, source_target_pairs={{0,1},{1,0},{2,3},{3,2},{4,5},{5,4},{6,7},{7,6},{8,9},{9,8},{10,11... | collective-permute-start | bytes 1376264 | tf_op jit(solution)/shard_map/ppermute | solution.py:18
  180.1 14.9 %collective-permute-start.38 = (bf16[896,256]{1,0:T(8,128)(2,1)}, bf16[896,256]{1,0:T(8,128)(2,1)}, u32[]{:S(2)}, u32[]{:S(2)}) collective-permute-start(bf16[896,256]{1,0:T(8,128)(2,1)} %collective-permute-done.28.refs_2_), channel_id=1, source_target_pairs={{0,1},{1,0},{2,3},{3,2},{4,5},{5,4},{6,7},{7,6},{8,9},{9,8},{10,11... | collective-permute-start | bytes 1376264 | tf_op jit(solution)/shard_map/ppermute | solution.py:18
  180.2 16.0 %collective-permute-start.39 = (bf16[896,256]{1,0:T(8,128)(2,1)}, bf16[896,256]{1,0:T(8,128)(2,1)}, u32[]{:S(2)}, u32[]{:S(2)}) collective-permute-start(bf16[896,256]{1,0:T(8,128)(2,1)} %collective-permute-done.30.refs_4_), channel_id=1, source_target_pairs={{0,1},{1,0},{2,3},{3,2},{4,5},{5,4},{6,7},{7,6},{8,9},{9,8},{10,11... | collective-permute-start | bytes 1376264 | tf_op jit(solution)/shard_map/ppermute | solution.py:18
  189.4 29.4 %collective-permute-start.45 = (bf16[1,128,256]{2,1,0:T(8,128)(2,1)S(1)}, bf16[1,128,256]{2,1,0:T(8,128)(2,1)S(1)}, u32[]{:S(2)}, u32[]{:S(2)}) collective-permute-start(bf16[1,128,256]{2,1,0:T(8,128)(2,1)S(1)} %get-tuple-element.95), channel_id=1, source_target_pairs={{0,8},{8,0},{16,24},{24,16},{1,9},{9,1},{17,25},{25,17},{2,10},{10... | collective-permute-start | bytes 196616 | tf_op jit(solution)/shard_map/ppermute | solution.py:18
  189.5 29.3 %collective-permute-start.46 = (bf16[1,128,256]{2,1,0:T(8,128)(2,1)S(1)}, bf16[1,128,256]{2,1,0:T(8,128)(2,1)S(1)}, u32[]{:S(2)}, u32[]{:S(2)}) collective-permute-start(bf16[1,128,256]{2,1,0:T(8,128)(2,1)S(1)} %get-tuple-element.96), channel_id=1, source_target_pairs={{0,16},{8,24},{16,0},{24,8},{1,17},{9,25},{17,1},{25,9},{2,18},{10... | collective-permute-start | bytes 196616 | tf_op jit(solution)/shard_map/ppermute | solution.py:18
  203.2 15.4 %collective-permute-start.42 = (bf16[2,128,256]{2,1,0:T(8,128)(2,1)S(1)}, bf16[2,128,256]{2,1,0:T(8,128)(2,1)S(1)}, u32[]{:S(2)}, u32[]{:S(2)}) collective-permute-start(bf16[2,128,256]{2,1,0:T(8,128)(2,1)S(1)} %get-tuple-element.89), channel_id=1, source_target_pairs={{0,24},{8,16},{16,8},{24,0},{1,25},{9,17},{17,9},{25,1},{2,26},{10... | collective-permute-start | bytes 393224 | tf_op jit(solution)/shard_map/ppermute | solution.py:18
  208.7 14.7 %collective-permute-start.37 = (bf16[128,256]{1,0:T(8,128)(2,1)S(1)}, bf16[128,256]{1,0:T(8,128)(2,1)S(1)}, u32[]{:S(2)}, u32[]{:S(2)}) collective-permute-start(bf16[128,256]{1,0:T(8,128)(2,1)S(1)} %fusion.7), channel_id=1, source_target_pairs={{0,7},{1,6},{2,5},{3,4},{4,3},{5,2},{6,1},{7,0},{8,15},{9,14},{10,... | collective-permute-start | bytes 196616 | tf_op jit(solution)/shard_map/ppermute | solution.py:18
  (54 other events, 350.8 us)

commit v3 on v2

--- a/solution.py
+++ b/solution.py
@@ -214,6 +214,74 @@
                 outs[z][number, side * size : (side + 1) * size] = total[z]
 
 
+def base_kernel(other_ref, piece_ref, out_ref):
+    tiles, rows, tile = other_ref.shape
+    half = rows // 2
+    for side in range(2):
+        start = (1 - side) * half
+        out_ref[side * half : (side + 1) * half] = sum(
+            jnp.dot(
+                other_ref[t, start : start + half],
+                piece_ref[t * tile : (t + 1) * tile],
+                preferred_element_type=jnp.float32,
+            )
+            for t in range(tiles)
+        )
+
+
+def base_call(other, piece):
+    rows, (inner, width) = other.shape[1], piece.shape
+    return pl.pallas_call(
+        base_kernel,
+        in_specs=[pl.BlockSpec(memory_space=pltpu.VMEM)] * 2,
+        out_specs=pl.BlockSpec(memory_space=pltpu.VMEM),
+        out_shape=jax.ShapeDtypeStruct((rows, width), jnp.float32),
+        compiler_params=pltpu.CompilerParams(vmem_limit_bytes=16 * 2**20),
+        cost_estimate=pl.CostEstimate(
+            flops=2 * rows * inner * width + 10**8,
+            bytes_accessed=2 * inner * width,
+            transcendentals=0,
+        ),
+        name="base",
+    )(other, piece)
+
+
+def last_kernel(blocks, own_ref, base_ref, piece_ref, *outs):
+    tiles, rows, tile = own_ref.shape
+    half = rows // 2
+    size = half // blocks
+    for side in range(2):
+        part = slice(side * half, (side + 1) * half)
+        total = base_ref[part] + sum(
+            jnp.dot(
+                own_ref[t, part],
+                piece_ref[t * tile : (t + 1) * tile],
+                preferred_element_type=jnp.float32,
+            )
+            for t in range(tiles)
+        )
+        total = total.astype(jnp.bfloat16).reshape(blocks, size, -1)
+        for z in range(blocks):
+            outs[z][0, side * size : (side + 1) * size] = total[z]
+
+
+def last_call(own, base, piece, blocks):
+    rows, (inner, width) = own.shape[1], piece.shape
+    out = jax.ShapeDtypeStruct((1, rows // blocks, width), jnp.bfloat16)
+    return pl.pallas_call(
+        functools.partial(last_kernel, blocks),
+        in_specs=[pl.BlockSpec(memory_space=pltpu.VMEM)] * 3,
+        out_specs=[pl.BlockSpec(memory_space=pltpu.VMEM)] * blocks,
+        out_shape=[out] * blocks,
+        compiler_params=pltpu.CompilerParams(vmem_limit_bytes=16 * 2**20),
+        cost_estimate=pl.CostEstimate(
+            flops=2 * rows * inner * width + 10**8,
+            bytes_accessed=2 * inner * width,
+            transcendentals=0,
+        ),
+    )(own, base, piece)
+
+
 def dots_call(own, other, own_pieces, other_pieces, blocks):
     rows = own.shape[1]
     inner, width = own_pieces[0].shape
@@ -317,7 +385,11 @@
         else:
             own_pieces = [down_pieces[2 * pair + 1] for pair in group]
             other_pieces = [swap(down_pieces[2 * pair], "tp", 1) for pair in group]
-        parts = dots_call(hidden, other_hidden, own_pieces, other_pieces, blocks)
+        if number == 2:
+            base = base_call(other_hidden, other_pieces[0])
+            parts = last_call(hidden, base, own_pieces[0], blocks)
+        else:
+            parts = dots_call(hidden, other_hidden, own_pieces, other_pieces, blocks)
         if direct:
             parts = [swap(part, "fs", z) for z, part in enumerate(parts)]
         else:

time: 226 us -> 224 us (level)
    pallas_call x3 -> x2, Pallas kernels: 4.83 us -> 3.09 us  [dots_call(): pl.pallas_call(functools.partial(dots_kernel, blocks), in_specs=[pl.Block...]
where the time goes in v3:
time: 224 us; the launch traced here: 223 us
  waiting for transfers between devices  80.3 us (36%)
  starting transfers between devices  77.7 us (35%)
  Pallas kernels  35.3 us (16%)
  local copies, waits for them, and re-layouts  20 us (9%)
  other arithmetic  6.22 us (3%)
    ppermute x48, waiting for transfers between devices, swap(): return lax.ppermute(value, axis, pairs)  80.3 us
    ppermute x48, starting transfers between devices, swap(): return lax.ppermute(value, axis, pairs)  77.7 us
    unnamed x77, local copies, waits for them, and re-layouts  17 us
    pallas_call x3, Pallas kernels, ready(): pl.pallas_call(functools.partial(ready_kernel, masks), in_specs=in_specs,...  15.6 us
    pallas_call x2, Pallas kernels, slab_call(): pl.pallas_call(functools.partial(kernel, len(pieces)), grid_spec=pltpu.Pr...  8.17 us
    pallas_call x2, Pallas kernels, fill_call(): pl.pallas_call(functools.partial(fill_kernel, masks), in_specs=in_specs,...  4.85 us
  transfers between devices with their start and end apart: 48, of which 15 were waited for; matrix products, arithmetic and copies ran while one was open for 4% of the time, Pallas kernels for 16%

profile of v3, /device:TPU:1, one launch (start us, length us, event | category | flops | bytes accessed | tf_op | source)
XLA Modules:
  0.0 222.5 jit_solution(16452753677126982362)
XLA Ops:
  2.3 2.1 collective-permute-start.14
  10.2 2.0 collective-permute-start.6
  14.8 1.9 collective-permute-start.2
  21.8 3.3 %collective-permute-start.9 = (bf16[64,2048]{1,0:T(8,128)(2,1)}, bf16[64,2048]{1,0:T(8,128)(2,1)S(1)}, u32[]{:S(2)}, u32[]{:S(2)}) collective-permute-start(bf16[64,2048]{1,0:T(8,128)(2,1)} %norm_rows.1), channel_id=1, source_target_pairs={{0,24},{8,16},{16,8},{24,0},{1,25},{9,17},{17,9},{25,1},{2,26},{10... | collective-permute-start | bytes 786440 | tf_op jit(solution)/shard_map/ppermute | solution.py:18
  26.6 4.9 %shard_map.102 = (bf16[896,256]{1,0:T(8,128)(2,1)}, bf16[896,256]{1,0:T(8,128)(2,1)}, bf16[896,256]{1,0:T(8,128)(2,1)}, bf16[896,256]{1,0:T(8,128)(2,1)}, bf16[8...) custom-call(s32[1]{0:T(128)} %bitcast.me_ref, f32[8,896,256]{2,1,0:T(8,128)} %master_ref.3, f32[1,256]{1,0:T(1,128)} %bitcast.90), custom_call_target="tpu_custom_call" | custom-call | flops 100000000 | bytes 8257536 | tf_op jit(solution)/shard_map/pallas_call | solution.py:77
  31.5 3.1 %collective-permute-start.11 = (bf16[896,256]{1,0:T(8,128)(2,1)}, bf16[896,256]{1,0:T(8,128)(2,1)S(1)}, u32[]{:S(2)}, u32[]{:S(2)}) collective-permute-start(bf16[896,256]{1,0:T(8,128)(2,1)} %get-tuple-element.53), channel_id=1, source_target_pairs={{0,1},{1,0},{2,3},{3,2},{4,5},{5,4},{6,7},{7,6},{8,9},{9,8},{10,11... | collective-permute-start | bytes 1376264 | tf_op jit(solution)/shard_map/ppermute | solution.py:18
  34.6 12.7 %collective-permute-done.8 = bf16[64,2048]{1,0:T(8,128)(2,1)S(1)} collective-permute-done((bf16[64,2048]{1,0:T(8,128)(2,1)}, bf16[64,2048]{1,0:T(8,128)(2,1)S(1)}, u32[]{:S(2)}, u32[]{:S(2)}) %collective-permute-start.8) | collective-permute-done | bytes 262176 | tf_op jit(solution)/shard_map/ppermute | solution.py:18
  47.3 2.4 %collective-permute-start.13 = (bf16[896,256]{1,0:T(8,128)(2,1)}, bf16[896,256]{1,0:T(8,128)(2,1)S(1)}, u32[]{:S(2)}, u32[]{:S(2)}) collective-permute-start(bf16[896,256]{1,0:T(8,128)(2,1)} %get-tuple-element.54), channel_id=1, source_target_pairs={{0,3},{1,2},{2,1},{3,0},{4,7},{5,6},{6,5},{7,4},{8,11},{9,10},{10,... | collective-permute-start | bytes 1376264 | tf_op jit(solution)/shard_map/ppermute | solution.py:18
  52.0 1.8 collective-permute-start.17
  53.8 5.7 %shard_map.104 = (bf16[896,256]{1,0:T(8,128)(2,1)}, bf16[896,256]{1,0:T(8,128)(2,1)}, bf16[896,256]{1,0:T(8,128)(2,1)}, bf16[896,256]{1,0:T(8,128)(2,1)}, bf16[8...) custom-call(s32[1]{0:T(128)} %bitcast.me_ref, ...), custom_call_target="tpu_custom_call" | custom-call | flops 100000000 | bytes 11010048 | tf_op jit(solution)/shard_map/pallas_call | solution.py:77
  64.4 7.3 %collective-permute-done.16.refs_6_ = bf16[896,256]{1,0:T(8,128)(2,1)S(1)} collective-permute-done((bf16[896,256]{1,0:T(8,128)(2,1)}, bf16[896,256]{1,0:T(8,128)(2,1)S(1)}, u32[]{:S(2)}, u32[]{:S(2)}) %collective-permute-start.16) | collective-permute-done | bytes 458784 | tf_op jit(solution)/shard_map/ppermute | solution.py:18
  72.4 10.4 %collective-permute-start.20 = (bf16[896,256]{1,0:T(8,128)(2,1)}, bf16[896,256]{1,0:T(8,128)(2,1)S(1)}, u32[]{:S(2)}, u32[]{:S(2)}) collective-permute-start(bf16[896,256]{1,0:T(8,128)(2,1)} %get-tuple-element.63), channel_id=1, source_target_pairs={{0,3},{1,2},{2,1},{3,0},{4,7},{5,6},{6,5},{7,4},{8,11},{9,10},{10,... | collective-permute-start | bytes 1376264 | tf_op jit(solution)/shard_map/ppermute | solution.py:18
  85.7 2.2 collective-permute-done.19.refs_2_
  87.9 8.2 %collective-permute-start.23 = (bf16[896,256]{1,0:T(8,128)(2,1)}, bf16[896,256]{1,0:T(8,128)(2,1)S(1)}, u32[]{:S(2)}, u32[]{:S(2)}) collective-permute-start(bf16[896,256]{1,0:T(8,128)(2,1)} %get-tuple-element.66), channel_id=1, source_target_pairs={{0,6},{1,7},{2,4},{3,5},{4,2},{5,3},{6,0},{7,1},{8,14},{9,15},{10,... | collective-permute-start | bytes 1376264 | tf_op jit(solution)/shard_map/ppermute | solution.py:18
  96.1 7.4 %collective-permute-done.20.refs_3_ = bf16[896,256]{1,0:T(8,128)(2,1)S(1)} collective-permute-done((bf16[896,256]{1,0:T(8,128)(2,1)}, bf16[896,256]{1,0:T(8,128)(2,1)S(1)}, u32[]{:S(2)}, u32[]{:S(2)}) %collective-permute-start.20) | collective-permute-done | bytes 458784 | tf_op jit(solution)/shard_map/ppermute | solution.py:18
  103.8 5.0 %shard_map.106 = (bf16[896,256]{1,0:T(8,128)(2,1)}, bf16[896,256]{1,0:T(8,128)(2,1)}, bf16[896,256]{1,0:T(8,128)(2,1)}, bf16[896,256]{1,0:T(8,128)(2,1)}, bf16[8...) custom-call(s32[1]{0:T(128)} %bitcast.me_ref, ...), custom_call_target="tpu_custom_call" | custom-call | flops 100000000 | bytes 11010048 | tf_op jit(solution)/shard_map/pallas_call | solution.py:77
  109.0 2.2 collective-permute-start.28
  117.3 4.1 %shard_map.103 = (bf16[1,896,2048]{2,1,0:T(8,128)(2,1)}, f32[2,512,448]{2,1,0:T(8,128)S(1)}) custom-call(s32[1]{0:T(128)} %bitcast.me_ref, bf16[256,2048]{1,0:T(8,128)(2,1)S(1)} %pad_maximum_fusion.mine_ref, bf16[256,2048]{1,0:T(8,128)(2,1)S(1)} %collective-permute-done.10.theirs_ref, bf16[896,256]{1,0:T(8,128)(2,1)S(1)} %copy-done.16, ...), custom_call_target="tpu_custom_call" | custom-call | flops 1979048192 | bytes 7340032 | tf_op jit(solution)/shard_map/pallas_call | solution.py:175
  121.4 14.7 %collective-permute-done.22.refs_5_ = bf16[896,256]{1,0:T(8,128)(2,1)S(1)} collective-permute-done((bf16[896,256]{1,0:T(8,128)(2,1)}, bf16[896,256]{1,0:T(8,128)(2,1)S(1)}, u32[]{:S(2)}, u32[]{:S(2)}) %collective-permute-start.22) | collective-permute-done | bytes 458784 | tf_op jit(solution)/shard_map/ppermute | solution.py:18
  142.5 4.0 %shard_map.105 = (bf16[1,896,2048]{2,1,0:T(8,128)(2,1)}, bf16[2,512,448]{2,1,0:T(8,128)(2,1)S(1)}) custom-call(s32[1]{0:T(128)} %bitcast.me_ref, bf16[256,2048]{1,0:T(8,128)(2,1)S(1)} %pad_maximum_fusion.mine_ref, bf16[256,2048]{1,0:T(8,128)(2,1)S(1)} %collective-permute-done.10.theirs_ref, f32[2,512,448]{2,1,0:T(8,128)S(1)} %get-tuple-element.59.act_ref, ...), custom_call_target="tpu_custom_call" | custom-call | flops 1979048192 | bytes 7340032 | tf_op jit(solution)/shard_map/pallas_call | solution.py:175
  151.3 18.8 %collective-permute-done.30.refs_4_ = bf16[896,256]{1,0:T(8,128)(2,1)} collective-permute-done((bf16[896,256]{1,0:T(8,128)(2,1)}, bf16[896,256]{1,0:T(8,128)(2,1)}, u32[]{:S(2)}, u32[]{:S(2)}) %collective-permute-start.30) | collective-permute-done | bytes 458784 | tf_op jit(solution)/shard_map/ppermute | solution.py:18
  171.6 8.5 %collective-permute-done.31.refs_5_.refs_1_ = bf16[896,256]{1,0:T(8,128)(2,1)S(1)} collective-permute-done((bf16[896,256]{1,0:T(8,128)(2,1)}, bf16[896,256]{1,0:T(8,128)(2,1)S(1)}, u32[]{:S(2)}, u32[]{:S(2)}) %collective-permute-start.31) | collective-permute-done | bytes 458784 | tf_op jit(solution)/shard_map/ppermute | solution.py:18
  180.6 2.7 %shard_map.107.refs_2_ = bf16[1,896,2048]{2,1,0:T(8,128)(2,1)} custom-call(s32[1]{0:T(128)} %bitcast.me_ref, bf16[896,256]{1,0:T(8,128)(2,1)S(1)} %copy-done.2, bf16[896,256]{1,0:T(8,128)(2,1)S(1)} %collective-permute-done.27.refs_1_, bf16[896,256]{1,0:T(8,128)(2,1)} %collective-permute-done.28.refs_2_, ...), custom_call_target="tpu_custom_call" | custom-call | flops 100000000 | bytes 5505024 | tf_op jit(solution)/shard_map/pallas_call | solution.py:147
  184.1 2.1 shard_map.108
  189.5 2.5 %collective-permute-start.46 = (bf16[1,128,256]{2,1,0:T(8,128)(2,1)S(1)}, bf16[1,128,256]{2,1,0:T(8,128)(2,1)S(1)}, u32[]{:S(2)}, u32[]{:S(2)}) collective-permute-start(bf16[1,128,256]{2,1,0:T(8,128)(2,1)S(1)} %get-tuple-element.96), channel_id=1, source_target_pairs={{0,16},{8,24},{16,0},{24,8},{1,17},{9,25},{17,1},{25,9},{2,18},{10... | collective-permute-start | bytes 196616 | tf_op jit(solution)/shard_map/ppermute | solution.py:18
  195.3 2.2 collective-permute-start.36
  197.5 2.4 %shard_map.110 = (bf16[2,128,256]{2,1,0:T(8,128)(2,1)S(1)}, bf16[2,128,256]{2,1,0:T(8,128)(2,1)S(1)}, bf16[2,128,256]{2,1,0:T(8,128)(2,1)S(1)}, bf16[2,128,256]{2,1,0:T(8,128)(2,1)S(1)}) custom-call(bf16[2,512,448]{2,1,0:T(8,128)(2,1)S(1)} %get-tuple-element.79.own_ref, bf16[2,512,448]{2,1,0:T(8,128)(2,1)S(1)} %copy.31.other_ref, ...), custom_call_target="tpu_custom_call" | custom-call | flops 1039524096 | bytes 1835008 | tf_op jit(solution)/shard_map/pallas_call | solution.py:290
  201.4 2.2 collective-permute-start.42
  203.6 2.2 %collective-permute-done.40 = bf16[2,128,256]{2,1,0:T(8,128)(2,1)S(1)} collective-permute-done((bf16[2,128,256]{2,1,0:T(8,128)(2,1)S(1)}, bf16[2,128,256]{2,1,0:T(8,128)(2,1)S(1)}, u32[]{:S(2)}, u32[]{:S(2)}) %collective-permute-start.40) | collective-permute-done | bytes 131104 | tf_op jit(solution)/shard_map/ppermute | solution.py:18
  205.8 2.7 %collective-permute-start.47 = (bf16[1,128,256]{2,1,0:T(8,128)(2,1)S(1)}, bf16[1,128,256]{2,1,0:T(8,128)(2,1)S(1)}, u32[]{:S(2)}, u32[]{:S(2)}) collective-permute-start(bf16[1,128,256]{2,1,0:T(8,128)(2,1)S(1)} %get-tuple-element.97), channel_id=1, source_target_pairs={{0,24},{8,16},{16,8},{24,0},{1,25},{9,17},{17,9},{25,1},{2,26},{10... | collective-permute-start | bytes 196616 | tf_op jit(solution)/shard_map/ppermute | solution.py:18
  208.5 8.4 %collective-permute-start.37 = (bf16[128,256]{1,0:T(8,128)(2,1)S(1)}, bf16[128,256]{1,0:T(8,128)(2,1)S(1)}, u32[]{:S(2)}, u32[]{:S(2)}) collective-permute-start(bf16[128,256]{1,0:T(8,128)(2,1)S(1)} %fusion.7), channel_id=1, source_target_pairs={{0,7},{1,6},{2,5},{3,4},{4,3},{5,2},{6,1},{7,0},{8,15},{9,14},{10,... | collective-permute-start | bytes 196616 | tf_op jit(solution)/shard_map/ppermute | solution.py:18
  219.1 2.0 collective-permute-done.44
  (189 shorter events, 59.3 us)
Async XLA Ops:
  2.3 47.4 %collective-permute-start.14 = (bf16[896,256]{1,0:T(8,128)(2,1)S(1)}, bf16[896,256]{1,0:T(8,128)(2,1)S(1)}, u32[]{:S(2)}, u32[]{:S(2)}) collective-permute-start(bf16[896,256]{1,0:T(8,128)(2,1)S(1)} %get-tuple-element.102), channel_id=1, source_target_pairs={{0,4},{1,5},{2,6},{3,7},{4,0},{5,1},{6,2},{7,3},{8,12},{9,13},{10,... | collective-permute-start | bytes 1376264 | tf_op jit(solution)/shard_map/ppermute | solution.py:18
  25.2 22.1 %collective-permute-start.8 = (bf16[64,2048]{1,0:T(8,128)(2,1)}, bf16[64,2048]{1,0:T(8,128)(2,1)S(1)}, u32[]{:S(2)}, u32[]{:S(2)}) collective-permute-start(bf16[64,2048]{1,0:T(8,128)(2,1)} %norm_rows.1), channel_id=1, source_target_pairs={{0,16},{8,24},{16,0},{24,8},{1,17},{9,25},{17,1},{25,9},{2,18},{10... | collective-permute-start | bytes 786440 | tf_op jit(solution)/shard_map/ppermute | solution.py:18
  25.2 24.5 %collective-permute-start.7 = (bf16[64,2048]{1,0:T(8,128)(2,1)}, bf16[64,2048]{1,0:T(8,128)(2,1)S(1)}, u32[]{:S(2)}, u32[]{:S(2)}) collective-permute-start(bf16[64,2048]{1,0:T(8,128)(2,1)} %norm_rows.1), channel_id=1, source_target_pairs={{0,8},{8,0},{16,24},{24,16},{1,9},{9,1},{17,25},{25,17},{2,10},{10... | collective-permute-start | bytes 786440 | tf_op jit(solution)/shard_map/ppermute | solution.py:18
  25.4 25.5 %collective-permute-start.12 = (bf16[896,256]{1,0:T(8,128)(2,1)S(1)}, bf16[896,256]{1,0:T(8,128)(2,1)S(1)}, u32[]{:S(2)}, u32[]{:S(2)}) collective-permute-start(bf16[896,256]{1,0:T(8,128)(2,1)S(1)} %get-tuple-element.103), channel_id=1, source_target_pairs={{0,2},{1,3},{2,0},{3,1},{4,6},{5,7},{6,4},{7,5},{8,10},{9,11},{10,... | collective-permute-start | bytes 1376264 | tf_op jit(solution)/shard_map/ppermute | solution.py:18
  31.5 20.6 %collective-permute-start.11 = (bf16[896,256]{1,0:T(8,128)(2,1)}, bf16[896,256]{1,0:T(8,128)(2,1)S(1)}, u32[]{:S(2)}, u32[]{:S(2)}) collective-permute-start(bf16[896,256]{1,0:T(8,128)(2,1)} %get-tuple-element.53), channel_id=1, source_target_pairs={{0,1},{1,0},{2,3},{3,2},{4,5},{5,4},{6,7},{7,6},{8,9},{9,8},{10,11... | collective-permute-start | bytes 1376264 | tf_op jit(solution)/shard_map/ppermute | solution.py:18
  47.3 13.9 %collective-permute-start.13 = (bf16[896,256]{1,0:T(8,128)(2,1)}, bf16[896,256]{1,0:T(8,128)(2,1)S(1)}, u32[]{:S(2)}, u32[]{:S(2)}) collective-permute-start(bf16[896,256]{1,0:T(8,128)(2,1)} %get-tuple-element.54), channel_id=1, source_target_pairs={{0,3},{1,2},{2,1},{3,0},{4,7},{5,6},{6,5},{7,4},{8,11},{9,10},{10,... | collective-permute-start | bytes 1376264 | tf_op jit(solution)/shard_map/ppermute | solution.py:18
  49.7 12.8 %collective-permute-start.15 = (bf16[896,256]{1,0:T(8,128)(2,1)}, bf16[896,256]{1,0:T(8,128)(2,1)S(1)}, u32[]{:S(2)}, u32[]{:S(2)}) collective-permute-start(bf16[896,256]{1,0:T(8,128)(2,1)} %get-tuple-element.55), channel_id=1, source_target_pairs={{0,5},{1,4},{2,7},{3,6},{4,1},{5,0},{6,3},{7,2},{8,13},{9,12},{10,... | collective-permute-start | bytes 1376264 | tf_op jit(solution)/shard_map/ppermute | solution.py:18
  49.7 21.9 %collective-permute-start.16 = (bf16[896,256]{1,0:T(8,128)(2,1)}, bf16[896,256]{1,0:T(8,128)(2,1)S(1)}, u32[]{:S(2)}, u32[]{:S(2)}) collective-permute-start(bf16[896,256]{1,0:T(8,128)(2,1)} %get-tuple-element.56), channel_id=1, source_target_pairs={{0,6},{1,7},{2,4},{3,5},{4,2},{5,3},{6,0},{7,1},{8,14},{9,15},{10,... | collective-permute-start | bytes 1376264 | tf_op jit(solution)/shard_map/ppermute | solution.py:18
  51.0 58.0 %collective-permute-start.10 = (bf16[256,2048]{1,0:T(8,128)(2,1)S(1)}, bf16[256,2048]{1,0:T(8,128)(2,1)S(1)}, u32[]{:S(2)}, u32[]{:S(2)}) collective-permute-start(bf16[256,2048]{1,0:T(8,128)(2,1)S(1)} %pad_maximum_fusion.mine_ref), channel_id=1, source_target_pairs={{0,1},{1,0},{2,3},{3,2},{4,5},{5,4},{6,7},{7,6},{8,9},{9,8},{10,11... | collective-permute-start | bytes 3145736 | tf_op jit(solution)/shard_map/ppermute | solution.py:18
  52.0 30.8 %collective-permute-start.17 = (bf16[896,256]{1,0:T(8,128)(2,1)}, bf16[896,256]{1,0:T(8,128)(2,1)S(1)}, u32[]{:S(2)}, u32[]{:S(2)}) collective-permute-start(bf16[896,256]{1,0:T(8,128)(2,1)} %get-tuple-element.57), channel_id=1, source_target_pairs={{0,7},{1,6},{2,5},{3,4},{4,3},{5,2},{6,1},{7,0},{8,15},{9,14},{10,... | collective-permute-start | bytes 1376264 | tf_op jit(solution)/shard_map/ppermute | solution.py:18
  62.0 23.4 %collective-permute-start.18 = (bf16[896,256]{1,0:T(8,128)(2,1)}, bf16[896,256]{1,0:T(8,128)(2,1)S(1)}, u32[]{:S(2)}, u32[]{:S(2)}) collective-permute-start(bf16[896,256]{1,0:T(8,128)(2,1)} %get-tuple-element.61), channel_id=1, source_target_pairs={{0,1},{1,0},{2,3},{3,2},{4,5},{5,4},{6,7},{7,6},{8,9},{9,8},{10,11... | collective-permute-start | bytes 1376264 | tf_op jit(solution)/shard_map/ppermute | solution.py:18
  63.2 24.7 %collective-permute-start.19 = (bf16[896,256]{1,0:T(8,128)(2,1)}, bf16[896,256]{1,0:T(8,128)(2,1)S(1)}, u32[]{:S(2)}, u32[]{:S(2)}) collective-permute-start(bf16[896,256]{1,0:T(8,128)(2,1)} %get-tuple-element.62), channel_id=1, source_target_pairs={{0,2},{1,3},{2,0},{3,1},{4,6},{5,7},{6,4},{7,5},{8,10},{9,11},{10,... | collective-permute-start | bytes 1376264 | tf_op jit(solution)/shard_map/ppermute | solution.py:18
  72.4 31.0 %collective-permute-start.20 = (bf16[896,256]{1,0:T(8,128)(2,1)}, bf16[896,256]{1,0:T(8,128)(2,1)S(1)}, u32[]{:S(2)}, u32[]{:S(2)}) collective-permute-start(bf16[896,256]{1,0:T(8,128)(2,1)} %get-tuple-element.63), channel_id=1, source_target_pairs={{0,3},{1,2},{2,1},{3,0},{4,7},{5,6},{6,5},{7,4},{8,11},{9,10},{10,... | collective-permute-start | bytes 1376264 | tf_op jit(solution)/shard_map/ppermute | solution.py:18
  83.6 25.2 %collective-permute-start.21 = (bf16[896,256]{1,0:T(8,128)(2,1)}, bf16[896,256]{1,0:T(8,128)(2,1)S(1)}, u32[]{:S(2)}, u32[]{:S(2)}) collective-permute-start(bf16[896,256]{1,0:T(8,128)(2,1)} %get-tuple-element.64), channel_id=1, source_target_pairs={{0,4},{1,5},{2,6},{3,7},{4,0},{5,1},{6,2},{7,3},{8,12},{9,13},{10,... | collective-permute-start | bytes 1376264 | tf_op jit(solution)/shard_map/ppermute | solution.py:18
  85.4 50.7 %collective-permute-start.22 = (bf16[896,256]{1,0:T(8,128)(2,1)}, bf16[896,256]{1,0:T(8,128)(2,1)S(1)}, u32[]{:S(2)}, u32[]{:S(2)}) collective-permute-start(bf16[896,256]{1,0:T(8,128)(2,1)} %get-tuple-element.65), channel_id=1, source_target_pairs={{0,5},{1,4},{2,7},{3,6},{4,1},{5,0},{6,3},{7,2},{8,13},{9,12},{10,... | collective-permute-start | bytes 1376264 | tf_op jit(solution)/shard_map/ppermute | solution.py:18
  87.9 50.0 %collective-permute-start.23 = (bf16[896,256]{1,0:T(8,128)(2,1)}, bf16[896,256]{1,0:T(8,128)(2,1)S(1)}, u32[]{:S(2)}, u32[]{:S(2)}) collective-permute-start(bf16[896,256]{1,0:T(8,128)(2,1)} %get-tuple-element.66), channel_id=1, source_target_pairs={{0,6},{1,7},{2,4},{3,5},{4,2},{5,3},{6,0},{7,1},{8,14},{9,15},{10,... | collective-permute-start | bytes 1376264 | tf_op jit(solution)/shard_map/ppermute | solution.py:18
  103.4 35.2 %collective-permute-start.24 = (bf16[896,256]{1,0:T(8,128)(2,1)}, bf16[896,256]{1,0:T(8,128)(2,1)S(1)}, u32[]{:S(2)}, u32[]{:S(2)}) collective-permute-start(bf16[896,256]{1,0:T(8,128)(2,1)} %get-tuple-element.67), channel_id=1, source_target_pairs={{0,7},{1,6},{2,5},{3,4},{4,3},{5,2},{6,1},{7,0},{8,15},{9,14},{10,... | collective-permute-start | bytes 1376264 | tf_op jit(solution)/shard_map/ppermute | solution.py:18
  108.8 39.2 %collective-permute-start.25 = (bf16[896,256]{1,0:T(8,128)(2,1)}, bf16[896,256]{1,0:T(8,128)(2,1)}, u32[]{:S(2)}, u32[]{:S(2)}) collective-permute-start(bf16[896,256]{1,0:T(8,128)(2,1)} %get-tuple-element.69), channel_id=1, source_target_pairs={{0,6},{1,7},{2,4},{3,5},{4,2},{5,3},{6,0},{7,1},{8,14},{9,15},{10,... | collective-permute-start | bytes 1376264 | tf_op jit(solution)/shard_map/ppermute | solution.py:18
  109.0 40.7 %collective-permute-start.28 = (bf16[896,256]{1,0:T(8,128)(2,1)}, bf16[896,256]{1,0:T(8,128)(2,1)}, u32[]{:S(2)}, u32[]{:S(2)}) collective-permute-start(bf16[896,256]{1,0:T(8,128)(2,1)} %get-tuple-element.73), channel_id=1, source_target_pairs={{0,2},{1,3},{2,0},{3,1},{4,6},{5,7},{6,4},{7,5},{8,10},{9,11},{10,... | collective-permute-start | bytes 1376264 | tf_op jit(solution)/shard_map/ppermute | solution.py:18
  136.9 12.9 %collective-permute-start.29 = (bf16[896,256]{1,0:T(8,128)(2,1)}, bf16[896,256]{1,0:T(8,128)(2,1)S(1)}, u32[]{:S(2)}, u32[]{:S(2)}) collective-permute-start(bf16[896,256]{1,0:T(8,128)(2,1)} %get-tuple-element.74), channel_id=1, source_target_pairs={{0,3},{1,2},{2,1},{3,0},{4,7},{5,6},{6,5},{7,4},{8,11},{9,10},{10,... | collective-permute-start | bytes 1376264 | tf_op jit(solution)/shard_map/ppermute | solution.py:18
  147.0 39.2 %collective-permute-start.32 = (bf16[2,512,448]{1,2,0:T(8,128)(2,1)S(1)}, bf16[2,512,448]{1,2,0:T(8,128)(2,1)}, u32[]{:S(2)}, u32[]{:S(2)}) collective-permute-start(bf16[2,512,448]{1,2,0:T(8,128)(2,1)S(1)} %copy.30), channel_id=1, source_target_pairs={{0,1},{1,0},{2,3},{3,2},{4,5},{5,4},{6,7},{7,6},{8,9},{9,8},{10,11... | collective-permute-start | bytes 2752520 | tf_op jit(solution)/shard_map/ppermute | solution.py:18
  147.9 22.1 %collective-permute-start.30 = (bf16[896,256]{1,0:T(8,128)(2,1)}, bf16[896,256]{1,0:T(8,128)(2,1)}, u32[]{:S(2)}, u32[]{:S(2)}) collective-permute-start(bf16[896,256]{1,0:T(8,128)(2,1)} %get-tuple-element.75), channel_id=1, source_target_pairs={{0,4},{1,5},{2,6},{3,7},{4,0},{5,1},{6,2},{7,3},{8,12},{9,13},{10,... | collective-permute-start | bytes 1376264 | tf_op jit(solution)/shard_map/ppermute | solution.py:18
  148.0 32.1 %collective-permute-start.31 = (bf16[896,256]{1,0:T(8,128)(2,1)}, bf16[896,256]{1,0:T(8,128)(2,1)S(1)}, u32[]{:S(2)}, u32[]{:S(2)}) collective-permute-start(bf16[896,256]{1,0:T(8,128)(2,1)} %get-tuple-element.76), channel_id=1, source_target_pairs={{0,5},{1,4},{2,7},{3,6},{4,1},{5,0},{6,3},{7,2},{8,13},{9,12},{10,... | collective-permute-start | bytes 1376264 | tf_op jit(solution)/shard_map/ppermute | solution.py:18
  149.7 30.5 %collective-permute-start.27 = (bf16[896,256]{1,0:T(8,128)(2,1)S(1)}, bf16[896,256]{1,0:T(8,128)(2,1)S(1)}, u32[]{:S(2)}, u32[]{:S(2)}) collective-permute-start(bf16[896,256]{1,0:T(8,128)(2,1)S(1)} %copy-done.7), channel_id=1, source_target_pairs={{0,1},{1,0},{2,3},{3,2},{4,5},{5,4},{6,7},{7,6},{8,9},{9,8},{10,11... | collective-permute-start | bytes 1376264 | tf_op jit(solution)/shard_map/ppermute | solution.py:18
  149.8 34.3 %collective-permute-start.26 = (bf16[896,256]{1,0:T(8,128)(2,1)}, bf16[896,256]{1,0:T(8,128)(2,1)S(1)}, u32[]{:S(2)}, u32[]{:S(2)}) collective-permute-start(bf16[896,256]{1,0:T(8,128)(2,1)} %get-tuple-element.70), channel_id=1, source_target_pairs={{0,7},{1,6},{2,5},{3,4},{4,3},{5,2},{6,1},{7,0},{8,15},{9,14},{10,... | collective-permute-start | bytes 1376264 | tf_op jit(solution)/shard_map/ppermute | solution.py:18
  170.1 21.9 %collective-permute-start.33 = (bf16[896,256]{1,0:T(8,128)(2,1)}, bf16[896,256]{1,0:T(8,128)(2,1)}, u32[]{:S(2)}, u32[]{:S(2)}) collective-permute-start(bf16[896,256]{1,0:T(8,128)(2,1)} %collective-permute-done.25.refs_0_), channel_id=1, source_target_pairs={{0,1},{1,0},{2,3},{3,2},{4,5},{5,4},{6,7},{7,6},{8,9},{9,8},{10,11... | collective-permute-start | bytes 1376264 | tf_op jit(solution)/shard_map/ppermute | solution.py:18
  180.1 14.0 %collective-permute-start.38 = (bf16[896,256]{1,0:T(8,128)(2,1)}, bf16[896,256]{1,0:T(8,128)(2,1)}, u32[]{:S(2)}, u32[]{:S(2)}) collective-permute-start(bf16[896,256]{1,0:T(8,128)(2,1)} %collective-permute-done.28.refs_2_), channel_id=1, source_target_pairs={{0,1},{1,0},{2,3},{3,2},{4,5},{5,4},{6,7},{7,6},{8,9},{9,8},{10,11... | collective-permute-start | bytes 1376264 | tf_op jit(solution)/shard_map/ppermute | solution.py:18
  180.2 15.1 %collective-permute-start.39 = (bf16[896,256]{1,0:T(8,128)(2,1)}, bf16[896,256]{1,0:T(8,128)(2,1)}, u32[]{:S(2)}, u32[]{:S(2)}) collective-permute-start(bf16[896,256]{1,0:T(8,128)(2,1)} %collective-permute-done.30.refs_4_), channel_id=1, source_target_pairs={{0,1},{1,0},{2,3},{3,2},{4,5},{5,4},{6,7},{7,6},{8,9},{9,8},{10,11... | collective-permute-start | bytes 1376264 | tf_op jit(solution)/shard_map/ppermute | solution.py:18
  189.4 27.6 %collective-permute-start.45 = (bf16[1,128,256]{2,1,0:T(8,128)(2,1)S(1)}, bf16[1,128,256]{2,1,0:T(8,128)(2,1)S(1)}, u32[]{:S(2)}, u32[]{:S(2)}) collective-permute-start(bf16[1,128,256]{2,1,0:T(8,128)(2,1)S(1)} %get-tuple-element.95), channel_id=1, source_target_pairs={{0,8},{8,0},{16,24},{24,16},{1,9},{9,1},{17,25},{25,17},{2,10},{10... | collective-permute-start | bytes 196616 | tf_op jit(solution)/shard_map/ppermute | solution.py:18
  189.5 27.6 %collective-permute-start.46 = (bf16[1,128,256]{2,1,0:T(8,128)(2,1)S(1)}, bf16[1,128,256]{2,1,0:T(8,128)(2,1)S(1)}, u32[]{:S(2)}, u32[]{:S(2)}) collective-permute-start(bf16[1,128,256]{2,1,0:T(8,128)(2,1)S(1)} %get-tuple-element.96), channel_id=1, source_target_pairs={{0,16},{8,24},{16,0},{24,8},{1,17},{9,25},{17,1},{25,9},{2,18},{10... | collective-permute-start | bytes 196616 | tf_op jit(solution)/shard_map/ppermute | solution.py:18
  201.4 15.5 %collective-permute-start.42 = (bf16[2,128,256]{2,1,0:T(8,128)(2,1)S(1)}, bf16[2,128,256]{2,1,0:T(8,128)(2,1)S(1)}, u32[]{:S(2)}, u32[]{:S(2)}) collective-permute-start(bf16[2,128,256]{2,1,0:T(8,128)(2,1)S(1)} %get-tuple-element.89), channel_id=1, source_target_pairs={{0,24},{8,16},{16,8},{24,0},{1,25},{9,17},{17,9},{25,1},{2,26},{10... | collective-permute-start | bytes 393224 | tf_op jit(solution)/shard_map/ppermute | solution.py:18
  208.5 13.1 %collective-permute-start.37 = (bf16[128,256]{1,0:T(8,128)(2,1)S(1)}, bf16[128,256]{1,0:T(8,128)(2,1)S(1)}, u32[]{:S(2)}, u32[]{:S(2)}) collective-permute-start(bf16[128,256]{1,0:T(8,128)(2,1)S(1)} %fusion.7), channel_id=1, source_target_pairs={{0,7},{1,6},{2,5},{3,4},{4,3},{5,2},{6,1},{7,0},{8,15},{9,14},{10,... | collective-permute-start | bytes 196616 | tf_op jit(solution)/shard_map/ppermute | solution.py:18
  (54 other events, 353.6 us)
